TPU v7x, 32 devices: a whole 2x2x4 slice. The times are simulated.
32 devices in a mesh: grp: 2 (over x), ep: 16 (over z, y, core).
Axes of the slice: x: 2, y: 2, z: 4, core: 2. Of those that a mesh axis runs over, the one named last changes fastest.
Arguments:
- tokens: bfloat16 [384, 2048], P(('grp', 'ep')), parts along dimension 0, may hold values from -6 to 6
- norm_gain: float32 [2048], replicated, may hold values from 0.1 to 1.9
- query_weight: bfloat16 [2048, 512], P('ep'), may hold values from -0.125 to 0.125
- key_weight: bfloat16 [2048, 512], P('ep'), may hold values from -0.125 to 0.125
- value_weight: bfloat16 [2048, 512], P('ep'), may hold values from -0.125 to 0.125
- outgate_weight: bfloat16 [2048, 512], P('ep'), may hold values from -0.125 to 0.125
- ingate_weight: bfloat16 [2048, 4], P('ep'), may hold values from -0.125 to 0.125
- forget_weight: bfloat16 [2048, 4], P('ep'), may hold values from -0.125 to 0.125
- ingate_bias: float32 [4], replicated, may hold values from -1 to 1
- forget_bias: float32 [4], replicated, may hold values from 0.5 to 4
- memory: float32 [384, 4, 128, 128], P(('grp', 'ep')), parts along dimension 0, may hold values from -4 to 4
- normalizer: float32 [384, 4, 128], P(('grp', 'ep')), parts along dimension 0, may hold values from -4 to 4
- stabilizer: float32 [384, 4], P(('grp', 'ep')), parts along dimension 0, may hold values from -1 to 2
- mixer_weight: bfloat16 [512, 2048], P(None, 'ep'), may hold values from -0.25 to 0.25
- moe_gain: float32 [2048], replicated, may hold values from 0.1 to 1.9
- expert_gate: bfloat16 [16, 2048, 512], P('ep'), may hold values from -0.125 to 0.125
- expert_up: bfloat16 [16, 2048, 512], P('ep'), may hold values from -0.125 to 0.125
- expert_down: bfloat16 [16, 512, 2048], P('ep'), may hold values from -0.25 to 0.25
- expert_index: int32 [384, 6], P(('grp', 'ep')), parts along dimension 0, may hold values from 0 to 15, as said below
- route_weights: float32 [384, 6], P(('grp', 'ep')), parts along dimension 0, may hold values from 0.1 to 1
Outputs:
- layer_out: bfloat16 [384, 2048], P(('grp', 'ep')), parts along dimension 0
- new_memory: float32 [384, 4, 128, 128], P(('grp', 'ep')), parts along dimension 0
- new_normalizer: float32 [384, 4, 128], P(('grp', 'ep')), parts along dimension 0
- new_stabilizer: float32 [384, 4], P(('grp', 'ep')), parts along dimension 0
There are 2 independent parts, one for each index of `grp`. A program takes and returns all parts, laid end to end along the dimension named above; an argument that names none is the same for every part. Nothing has to cross between parts.
Inputs may be any that keep to these rules, and one draw needn't show every extreme that they name: `expert_index`: experts 0 to 15 form two groups of 8 consecutive numbers; each row names 6 different experts of one group. Among the 12 rows of one device at most 5 name one expert, and in every device some expert is named by exactly 5 of them.
All inputs are finite; a program needn't handle non-finite values.
Results may differ from a plain program's by a relative error of at most 0.013.
Values may be sent and summed in bfloat16 or wider, within the bound.
No kernel may reach another device: no remote copies, remote signals or barrier semaphores. Data moves between devices by JAX's collectives and lax.ppermute only.
A program may use at most 128 MiB of HBM per device.

v0:
```python
import jax
import jax.numpy as jnp
from jax import lax
from jax.sharding import PartitionSpec as P

M_HEAD_DIM = 128


EPS = 1e-06


def rms_normed(values, gain):
    scale = lax.rsqrt(jnp.mean(values * values, axis=-1, keepdims=True) + EPS)
    return values * scale * gain


def on_device(
    tokens,
    norm_gain,
    query_weight,
    key_weight,
    value_weight,
    outgate_weight,
    ingate_weight,
    forget_weight,
    ingate_bias,
    forget_bias,
    memory,
    normalizer,
    stabilizer,
    mixer_weight,
    moe_gain,
    expert_gate,
    expert_up,
    expert_down,
    expert_index,
    route_weights,
):
    f32 = jnp.float32
    bf16 = jnp.bfloat16
    ep_size = lax.axis_size("ep")
    seq_count = tokens.shape[0]
    model_width = tokens.shape[1]
    cell_width = query_weight.shape[1]
    head_count = ingate_bias.shape[0]
    stream = tokens.astype(f32)
    weight_list = (
        query_weight,
        key_weight,
        value_weight,
        outgate_weight,
        ingate_weight,
        forget_weight,
    )
    normed = rms_normed(stream, norm_gain).astype(bf16)
    normed_cols = lax.all_to_all(normed, "ep", split_axis=1, concat_axis=0, tiled=True)
    joined = jnp.concatenate(weight_list, axis=1)
    projected = lax.psum_scatter(
        jnp.dot(normed_cols, joined, preferred_element_type=f32),
        "ep",
        scatter_dimension=0,
        tiled=True,
    )
    query_sum = projected[:, :cell_width]
    key_sum = projected[:, cell_width : 2 * cell_width]
    value_sum = projected[:, 2 * cell_width : 3 * cell_width]
    outgate_sum = projected[:, 3 * cell_width : 4 * cell_width]
    ingate_sum = projected[:, 4 * cell_width : 4 * cell_width + head_count]
    forget_sum = projected[:, 4 * cell_width + head_count :]
    shape = (seq_count, head_count, M_HEAD_DIM)
    query_heads = query_sum.astype(bf16).astype(f32).reshape(shape)
    key_heads = key_sum.astype(bf16).astype(f32).reshape(shape) * M_HEAD_DIM ** (-0.5)
    value_heads = value_sum.astype(bf16).astype(f32).reshape(shape)
    outgate = outgate_sum.astype(bf16).astype(f32)
    ingate_pre = ingate_sum + ingate_bias
    forget_pre = forget_sum + forget_bias
    log_forget = jax.nn.log_sigmoid(forget_pre)
    new_stabilizer = jnp.maximum(log_forget + stabilizer, ingate_pre)
    keep = jnp.exp(log_forget + stabilizer - new_stabilizer)
    write = jnp.exp(ingate_pre - new_stabilizer)
    new_memory = (
        keep[..., None, None] * memory
        + write[..., None, None] * key_heads[..., :, None] * value_heads[..., None, :]
    )
    new_normalizer = keep[..., None] * normalizer + write[..., None] * key_heads
    numer = jnp.einsum("thd,thde->the", query_heads, new_memory, precision=lax.Precision.HIGHEST)
    denom = jnp.sum(query_heads * new_normalizer, axis=-1)
    hidden = numer / jnp.maximum(jnp.abs(denom), 1.0)[..., None]
    cell_out = (hidden.reshape(seq_count, cell_width) * jax.nn.sigmoid(outgate)).astype(bf16)
    mixed_cols = jnp.dot(
        lax.all_gather(cell_out, "ep", axis=0, tiled=True), mixer_weight, preferred_element_type=f32
    ).astype(bf16)
    mixed = lax.all_to_all(mixed_cols, "ep", split_axis=0, concat_axis=1, tiled=True)
    resid = stream + mixed.astype(f32)
    moe_in = rms_normed(resid, moe_gain).astype(bf16)
    local_experts = expert_gate.shape[0]
    expert_count = local_experts * ep_size
    chosen_k = expert_index.shape[1]
    group_width = expert_count // 2
    capacity = max(2, ((seq_count + 1) // 2 * chosen_k + group_width - 1) // group_width)
    routes = expert_index.reshape(-1)
    matches = (routes[:, None] == jnp.arange(expert_count, dtype=jnp.int32)[None, :]).astype(
        jnp.int32
    )
    slots = jnp.sum((jnp.cumsum(matches, axis=0) - 1) * matches, axis=1)
    target = routes * capacity + slots
    placing = (
        jnp.arange(expert_count * capacity, dtype=jnp.int32)[:, None] == target[None, :]
    ).astype(bf16)
    route_rows = jnp.repeat(moe_in, chosen_k, axis=0)
    outgoing = jnp.dot(placing, route_rows, preferred_element_type=f32).astype(bf16)
    outgoing = outgoing.reshape(expert_count, capacity, model_width)
    received = lax.all_to_all(outgoing, "ep", split_axis=0, concat_axis=0, tiled=True)
    count = received.shape[1]
    grouped = received.reshape(ep_size, local_experts, count, model_width)
    gate = jnp.einsum("sxcd,xdf->sxcf", grouped, expert_gate, preferred_element_type=f32)
    upward = jnp.einsum("sxcd,xdf->sxcf", grouped, expert_up, preferred_element_type=f32)
    inner = (jax.nn.silu(gate) * upward).astype(bf16)
    result = jnp.einsum("sxcf,xfd->sxcd", inner, expert_down, preferred_element_type=f32).astype(
        bf16
    )
    result = result.reshape(ep_size * local_experts, count, model_width)
    returned = lax.all_to_all(result, "ep", split_axis=0, concat_axis=0, tiled=True)
    flat_back = returned.reshape(expert_count * capacity, model_width)
    picked = jnp.dot(placing.T, flat_back, preferred_element_type=f32)
    weighted = picked * route_weights.reshape(-1)[:, None]
    combined = jnp.sum(weighted.reshape(seq_count, chosen_k, model_width), axis=1)
    layer_out = (resid + combined).astype(bf16)
    return (layer_out, new_memory, new_normalizer, new_stabilizer)


def solution(mesh):
    return jax.shard_map(
        on_device,
        mesh=mesh,
        in_specs=(
            P(("grp", "ep"), None),
            P(),
            P("ep", None),
            P("ep", None),
            P("ep", None),
            P("ep", None),
            P("ep", None),
            P("ep", None),
            P(),
            P(),
            P(("grp", "ep"), None, None, None),
            P(("grp", "ep"), None, None),
            P(("grp", "ep"), None),
            P(None, "ep"),
            P(),
            P("ep", None, None),
            P("ep", None, None),
            P("ep", None, None),
            P(("grp", "ep"), None),
            P(("grp", "ep"), None),
        ),
        out_specs=(
            P(("grp", "ep"), None),
            P(("grp", "ep"), None, None, None),
            P(("grp", "ep"), None, None),
            P(("grp", "ep"), None),
        ),
        check_vma=False,
    )
```

profile of v0, /device:TPU:0, one launch (start us, length us, event | category | flops | bytes accessed | tf_op | source)
XLA Modules:
  0.0 214.0 jit_solution(910980491938122106)
XLA Ops:
  7.2 1.1 fusion.30
  8.3 0.9 fusion.32
  9.9 7.4 %all-to-all-start = ((bf16[12,16,128]{2,0,1:T(8,128)(2,1)}), bf16[12,16,128]{2,0,1:T(8,128)(2,1)S(1)}, u32[]{:S(2)}, u32[]{:S(2)}) async-start(bf16[12,16,128]{2,0,1:T(8,128)(2,1)} %copy.51), calls=%async_computation | async-start | bytes 131072 | tf_op jit(solution)/shard_map/all_to_all | solution.py:56
  19.0 1.2 concatenate.3
  20.2 4.0 %all-to-all-done = bf16[12,16,128]{2,0,1:T(8,128)(2,1)S(1)} async-done(((bf16[12,16,128]{2,0,1:T(8,128)(2,1)}), bf16[12,16,128]{2,0,1:T(8,128)(2,1)S(1)}, u32[]{:S(2)}, u32[]{:S(2)}) %all-to-all-start) | async-done | bytes 49184 | tf_op jit(solution)/shard_map/all_to_all | solution.py:56
  24.3 1.5 fusion.44
  27.8 92.5 %all-reduce.3.cloned.1.call-done = f32[192,2056]{1,0:T(8,128)} async-done(((f32[192,2056]{1,0:T(8,128)}), f32[192,2056]{1,0:T(8,128)}) %all-reduce.3.cloned.1.call-update) | async-done | bytes 1579024
  120.2 0.9 dynamic-slice_convert_fusion
  121.3 0.9 subtract_exponential_fusion
  123.7 2.5 %multiply_add_fusion = f32[12,4,128,128]{3,2,1,0:T(8,128)S(1)} fusion(f32[12,4,128,128]{3,2,1,0:T(8,128)} %param.30, f32[12,4,128]{2,1,0:T(4,128)S(1)} %reshape.131, f32[12,4,128]{2,1,0:T(4,128)S(1)} %get-tuple-element.22, f32[12,4]{1,0:T(8,128)S(1)} %get-tuple-element.23), kind=kLoop, calls=%fused_computation | loop fusion | flops 2359296 | bytes 6340800 | tf_op jit(solution)/shard_map/add | solution.py:82
  126.2 1.7 copy-done.1
  127.8 1.5 fusion.45
  129.5 20.0 %all-gather = bf16[16,12,512]{2,1,0:T(8,128)(2,1)S(1)} all-gather(bf16[1,12,512]{2,1,0:T(8,128)(2,1)S(1)} %fusion.37), channel_id=1, replica_groups=mesh['grp'=2,'ep'=16] {'ep'}, dimensions={0}, use_global_device_ids=true | all-gather | bytes 208896 | tf_op jit(solution)/shard_map/all_gather | solution.py:91
  150.5 3.5 %all-to-all-start.1 = ((bf16[16,12,128]{2,1,0:T(8,128)(2,1)}), bf16[16,12,128]{2,1,0:T(8,128)(2,1)S(1)}, u32[]{:S(2)}, u32[]{:S(2)}) async-start(bf16[16,12,128]{2,1,0:T(8,128)(2,1)} %all_to_all.34), calls=%async_computation.1 | async-start | bytes 131072 | tf_op jit(solution)/shard_map/all_to_all | solution.py:93
  154.0 6.8 %all-to-all-done.1 = bf16[16,12,128]{2,1,0:T(8,128)(2,1)S(1)} async-done(((bf16[16,12,128]{2,1,0:T(8,128)(2,1)}), bf16[16,12,128]{2,1,0:T(8,128)(2,1)S(1)}, u32[]{:S(2)}, u32[]{:S(2)}) %all-to-all-start.1) | async-done | bytes 49184 | tf_op jit(solution)/shard_map/all_to_all | solution.py:93
  162.2 16.9 %all_to_all.42 = bf16[16,5,2048]{2,1,0:T(8,128)(2,1)S(1)} all-to-all(bf16[16,5,2048]{2,1,0:T(8,128)(2,1)S(1)} %reshape.122), channel_id=1, replica_groups=mesh['grp'=2,'ep'=16] {'ep'}, dimensions={0} | all-to-all | bytes 655360 | tf_op jit(solution)/shard_map/all_to_all | solution.py:113
  179.1 2.1 fusion.5
  181.3 2.6 %convolution_convert_fusion = bf16[16,5,2048]{2,0,1:T(8,128)(2,1)S(1)} fusion(bf16[1,512,2048]{2,1,0:T(8,128)(2,1)S(1)} %copy-done, bf16[1,2048,512]{2,1,0:T(8,128)(2,1)} %param.36, bf16[16,5,2048]{2,1,0:T(8,128)(2,1)S(1)} %all_to_all.42, f32[16,1,5,512]{3,0,2,1:T(8,128)S(1)} %fusion.5), kind=kOutput, calls=%fused_computation.2 | convolution fusion | flops 335953920 | bytes 5013504 | tf_op jit(solution)/shard_map/sxcf,xfd->sxcd/dot_general | solution.py:119
  183.8 1.0 copy.59
  184.8 4.1 %all-to-all-start.3 = ((bf16[16,5,2048]{2,1,0:T(8,128)(2,1)}), bf16[16,5,2048]{2,1,0:T(8,128)(2,1)S(1)}, u32[]{:S(2)}, u32[]{:S(2)}) async-start(bf16[16,5,2048]{2,1,0:T(8,128)(2,1)} %copy.59), calls=%async_computation.3 | async-start | bytes 1048576 | tf_op jit(solution)/shard_map/all_to_all | solution.py:123
  189.8 13.4 %all-to-all-done.3 = bf16[16,5,2048]{2,1,0:T(8,128)(2,1)S(1)} async-done(((bf16[16,5,2048]{2,1,0:T(8,128)(2,1)}), bf16[16,5,2048]{2,1,0:T(8,128)(2,1)S(1)}, u32[]{:S(2)}, u32[]{:S(2)}) %all-to-all-start.3) | async-done | bytes 327712 | tf_op jit(solution)/shard_map/all_to_all | solution.py:123
  203.2 0.9 reshape.127
  204.1 1.3 convolution_multiply_fusion
  205.6 1.6 add_convert_fusion
  (73 shorter events, 8.7 us)
Async XLA Ops:
  7.2 174.1 %copy-start = (bf16[1,512,2048]{2,1,0:T(8,128)(2,1)S(1)}, bf16[1,512,2048]{2,1,0:T(8,128)(2,1)}, u32[]{:S(2)}) copy-start(bf16[1,512,2048]{2,1,0:T(8,128)(2,1)} %param.37) | copy-start | bytes 6291460
  9.9 14.3 %all-to-all-start = ((bf16[12,16,128]{2,0,1:T(8,128)(2,1)}), bf16[12,16,128]{2,0,1:T(8,128)(2,1)S(1)}, u32[]{:S(2)}, u32[]{:S(2)}) async-start(bf16[12,16,128]{2,0,1:T(8,128)(2,1)} %copy.51), calls=%async_computation | async-start | bytes 131072 | tf_op jit(solution)/shard_map/all_to_all | solution.py:56
  17.3 102.9 %all-reduce.3.cloned.1.call-start = ((), (), s32[]{:S(2)}) async-start(), calls=%async_computation.4 | async-start | bytes 3342336
  20.2 5.7 %copy-start.10 = (f32[12,4]{0,1:T(4,128)S(1)}, f32[12,4]{0,1:T(4,128)}, u32[]{:S(2)}) copy-start(f32[12,4]{0,1:T(4,128)} %param.32) | copy-start | bytes 580
  20.2 5.8 %copy-start.7 = (s32[12,6]{0,1:T(8,128)S(1)}, s32[12,6]{0,1:T(8,128)}, u32[]{:S(2)}) copy-start(s32[12,6]{0,1:T(8,128)} %param.38) | copy-start | bytes 868
  20.2 5.9 %copy-start.12 = (u32[32]{0:T(128)S(1)}, u32[32]{0:T(128)}, u32[]{:S(2)}) copy-start(u32[32]{0:T(128)} %constant.40) | copy-start | bytes 388
  24.3 97.0 %copy-start.9 = (f32[4]{0:T(128)S(1)}, f32[4]{0:T(128)}, u32[]{:S(2)}) copy-start(f32[4]{0:T(128)} %param.28) | copy-start | bytes 52
  24.3 97.0 %copy-start.11 = (f32[4]{0:T(128)S(1)}, f32[4]{0:T(128)}, u32[]{:S(2)}) copy-start(f32[4]{0:T(128)} %param.29) | copy-start | bytes 52
  24.3 98.7 %copy-start.5 = (f32[12,4,128]{2,1,0:T(4,128)S(1)}, f32[12,4,128]{2,1,0:T(4,128)}, u32[]{:S(2)}) copy-start(f32[12,4,128]{2,1,0:T(4,128)} %param.31) | copy-start | bytes 73732
  126.2 1.7 copy-start.1
  127.8 21.8 %copy-start.4 = (bf16[512,128]{1,0:T(8,128)(2,1)S(1)}, bf16[512,128]{1,0:T(8,128)(2,1)}, u32[]{:S(2)}) copy-start(bf16[512,128]{1,0:T(8,128)(2,1)} %param.33) | copy-start | bytes 393220
  127.8 33.1 %copy-start.3 = (bf16[12,2048]{1,0:T(8,128)(2,1)S(1)}, bf16[12,2048]{1,0:T(8,128)(2,1)}, u32[]{:S(2)}) copy-start(bf16[12,2048]{1,0:T(8,128)(2,1)} %param.20) | copy-start | bytes 147460
  129.4 32.2 %copy-start.6 = (f32[2048]{0:T(1024)S(1)}, f32[2048]{0:T(1024)}, u32[]{:S(2)}) copy-start(f32[2048]{0:T(1024)} %param.34) | copy-start | bytes 24580
  150.5 10.4 %all-to-all-start.1 = ((bf16[16,12,128]{2,1,0:T(8,128)(2,1)}), bf16[16,12,128]{2,1,0:T(8,128)(2,1)S(1)}, u32[]{:S(2)}, u32[]{:S(2)}) async-start(bf16[16,12,128]{2,1,0:T(8,128)(2,1)} %all_to_all.34), calls=%async_computation.1 | async-start | bytes 131072 | tf_op jit(solution)/shard_map/all_to_all | solution.py:93
  161.0 0.6 copy-start.2
  181.3 7.7 %copy-start.8 = (f32[12,6]{0,1:T(8,128)S(1)}, f32[12,6]{0,1:T(8,128)}, u32[]{:S(2)}) copy-start(f32[12,6]{0,1:T(8,128)} %param.39) | copy-start | bytes 868
  184.8 18.4 %all-to-all-start.3 = ((bf16[16,5,2048]{2,1,0:T(8,128)(2,1)}), bf16[16,5,2048]{2,1,0:T(8,128)(2,1)S(1)}, u32[]{:S(2)}, u32[]{:S(2)}) async-start(bf16[16,5,2048]{2,1,0:T(8,128)(2,1)} %copy.59), calls=%async_computation.3 | async-start | bytes 1048576 | tf_op jit(solution)/shard_map/all_to_all | solution.py:123
Sparse Core Ops, SparseCore 0:
  26.0 94.2 all-reduce.2
where the time goes:
time: 215 us; the launch traced here: 214 us
  waiting for transfers between devices  117 us (54%)
  blocking collectives  36.9 us (17%)
  starting transfers between devices  15.1 us (7%)
  between operations  15.1 us (7%)
  local copies, waits for them, and re-layouts  11.4 us (5%)
  other arithmetic  9.43 us (4%)
  matrix products  9.42 us (4%)
    unnamed x2, waiting for transfers between devices  92.5 us
    all_gather x1, blocking collectives, on_device(): lax.all_gather(cell_out, 'ep', axis=0, tiled=True)  20 us
    all_to_all x1, blocking collectives, on_device(): lax.all_to_all(outgoing, 'ep', split_axis=0, concat_axis=0, tiled=True)  16.9 us
    all_to_all x1, waiting for transfers between devices, on_device(): lax.all_to_all(result, 'ep', split_axis=0, concat_axis=0, tiled=True)  13.4 us
    all_to_all x1, starting transfers between devices, on_device(): lax.all_to_all(normed, 'ep', split_axis=1, concat_axis=0, tiled=True)  7.41 us
    all_to_all x1, waiting for transfers between devices, on_device(): lax.all_to_all(mixed_cols, 'ep', split_axis=0, concat_axis=1, tiled=True)  6.85 us
    unnamed x39, local copies, waits for them, and re-layouts  5.48 us
  transfers between devices with their start and end apart: 4, of which 4 were waited for; matrix products, arithmetic and copies ran while one was open for 2% of the time, Pallas kernels for 0%

commit v1 on v0

--- a/solution.py
+++ b/solution.py
@@ -1,7 +1,12 @@
+import functools
+
 import jax
 import jax.numpy as jnp
 from jax import lax
+from jax.experimental import pallas as pl
+from jax.experimental.pallas import tpu as pltpu
 from jax.sharding import PartitionSpec as P
+
 
 M_HEAD_DIM = 128
 
@@ -14,7 +19,7 @@
     return values * scale * gain
 
 
-def on_device(
+def on_device_general(
     tokens,
     norm_gain,
     query_weight,
@@ -129,37 +134,475 @@
     return (layer_out, new_memory, new_normalizer, new_stabilizer)
 
 
+ARG_SPECS = (
+    P(("grp", "ep"), None),
+    P(),
+    P("ep", None),
+    P("ep", None),
+    P("ep", None),
+    P("ep", None),
+    P("ep", None),
+    P("ep", None),
+    P(),
+    P(),
+    P(("grp", "ep"), None, None, None),
+    P(("grp", "ep"), None, None),
+    P(("grp", "ep"), None),
+    P(None, "ep"),
+    P(),
+    P("ep", None, None),
+    P("ep", None, None),
+    P("ep", None, None),
+    P(("grp", "ep"), None),
+    P(("grp", "ep"), None),
+)
+OUT_SPECS = (
+    P(("grp", "ep"), None),
+    P(("grp", "ep"), None, None, None),
+    P(("grp", "ep"), None, None),
+    P(("grp", "ep"), None),
+)
+
+
+def swap(value, bit):
+    size = lax.axis_size("ep")
+    return lax.ppermute(value, "ep", [(i, i ^ bit) for i in range(size)])
+
+
+F32 = jnp.float32
+BF16 = jnp.bfloat16
+LANES = 128
+
+
+def local_call(kernel, outs, scratch=(), flops=1, moved=1, smem=(), hbm=(), anywhere=(), outs_hbm=(), limit=8):
+    def call(*args):
+        def space(i):
+            if i in smem:
+                return pltpu.SMEM
+            if i in hbm:
+                return pltpu.HBM
+            return pl.ANY if i in anywhere else pltpu.VMEM
+
+        specs = [pl.BlockSpec(memory_space=space(i)) for i in range(len(args))]
+        return pl.pallas_call(
+            kernel,
+            out_shape=[jax.ShapeDtypeStruct(*o) for o in outs],
+            in_specs=specs,
+            out_specs=[
+                pl.BlockSpec(memory_space=pltpu.HBM if i in outs_hbm else pltpu.VMEM)
+                for i in range(len(outs))
+            ],
+            scratch_shapes=list(scratch),
+            compiler_params=pltpu.CompilerParams(vmem_limit_bytes=limit * 2**20),
+            cost_estimate=pl.CostEstimate(
+                flops=flops, bytes_accessed=moved, transcendentals=0
+            ),
+        )(*args)
+
+    return call
+
+
+def stack_kernel(first, second, out, sems):
+    count = first.shape[0]
+    copies = [
+        pltpu.make_async_copy(first, out.at[:count], sems.at[0]),
+        pltpu.make_async_copy(second, out.at[count:], sems.at[1]),
+    ]
+    for copy in copies:
+        copy.start()
+    for copy in copies:
+        copy.wait()
+
+
+def stack(first, second):
+    shape = (first.shape[0] + second.shape[0],) + first.shape[1:]
+    return local_call(
+        stack_kernel,
+        [(shape, first.dtype)],
+        scratch=[pltpu.SemaphoreType.DMA((2,))],
+        anywhere=(0, 1),
+        limit=60,
+        moved=2 * first.size * 4,
+    )(first, second)[0]
+
+
+def join_kernel(
+    tokens, query, key, value, outgate, ingate, forget, joined, columns, turned, held, narrow, sems
+):
+    width = query.shape[1]
+    heads = ingate.shape[0]
+    copies = [
+        pltpu.make_async_copy(ingate, narrow.at[0], sems.at[0]),
+        pltpu.make_async_copy(forget, narrow.at[1], sems.at[1]),
+        pltpu.make_async_copy(tokens, held, sems.at[2]),
+    ]
+    for i, ref in enumerate((query, key, value, outgate)):
+        copies.append(
+            pltpu.make_async_copy(ref, joined.at[:, i * width : (i + 1) * width], sems.at[3 + i])
+        )
+    for copy in copies:
+        copy.start()
+    turned[...] = jnp.zeros_like(turned)
+    for copy in copies[:3]:
+        copy.wait()
+    turned[:heads] = narrow[0].astype(F32)
+    turned[heads : 2 * heads] = narrow[1].astype(F32)
+    joined[:, 4 * width :] = turned[...].T.astype(BF16)
+    part = columns.shape[2]
+    for z in range(columns.shape[0]):
+        columns[z] = held[:, z * part : (z + 1) * part]
+    for copy in copies[3:]:
+        copy.wait()
+
+
+def project_kernel(columns, gain, own, core, side, cross, out, scaled, weights, total, sems):
+    stations, rows, part = columns.shape
+    depth = own.shape[0]
+    copies = [
+        pltpu.make_async_copy(ref, weights.at[i], sems.at[i])
+        for i, ref in enumerate((own, core, side, cross))
+    ]
+    for copy in copies:
+        copy.start()
+    me = lax.axis_index("ep")
+    station, place = me // 4, me % 4
+    gain_here = gain[:, pl.ds(pl.multiple_of(station * part, LANES), part)]
+    for z in range(stations):
+        scaled[z * rows : (z + 1) * rows, :] = columns[z].astype(F32) * gain_here
+    width = out.shape[2]
+    step = 4 * LANES
+    for bits, copy in enumerate(copies):
+        start = pl.multiple_of((place ^ bits) * depth, LANES)
+        part_x = scaled[:, pl.ds(start, depth)].astype(BF16)
+        copy.wait()
+        for low in range(0, width, step):
+            high = min(low + step, width)
+            term = jnp.dot(part_x, weights[bits, :, low:high], preferred_element_type=F32)
+            if bits:
+                term = term + total[:, low:high]
+            if bits < 3:
+                total[:, low:high] = term
+            else:
+                for z in range(stations):
+                    out[z, :, low:high] = term[z * rows : (z + 1) * rows].astype(BF16)
+
+
+def rounded(value):
+    return value.astype(BF16).astype(F32)
+
+
+def cell_kernel(
+    ingate_bias, forget_bias, received, tokens, memory, normalizer, stabilizer,
+    new_memory, new_normalizer, new_stabilizer, cell_out,
+    turned, flipped, keeps, numer, fresh, sems,
+):
+    stations, rows, _ = received.shape
+    heads = memory.shape[1]
+    dim = memory.shape[2]
+    width = heads * dim
+    stream = tokens[...].astype(F32)
+    scale = lax.rsqrt(jnp.mean(stream * stream, axis=-1, keepdims=True) + EPS)
+    total = received[0].astype(F32)
+    for z in range(1, stations):
+        total = total + received[z].astype(F32)
+    total = total * scale
+    gates = total[:, 4 * width :]
+    value = rounded(total[:, 2 * width : 3 * width])
+    lane = lax.broadcasted_iota(jnp.int32, (rows, heads), 1)
+    states = jnp.zeros((rows, heads), F32)
+    denoms = []
+    for h in range(heads):
+        cut = slice(h * dim, (h + 1) * dim)
+        query = rounded(total[:, h * dim : (h + 1) * dim])
+        key = rounded(total[:, width + h * dim : width + (h + 1) * dim]) * dim ** (-0.5)
+        ingate_pre = gates[:, h : h + 1] + ingate_bias[h]
+        forget_pre = gates[:, heads + h : heads + h + 1] + forget_bias[h]
+        log_forget = jnp.minimum(forget_pre, 0.0) - jnp.log1p(jnp.exp(-jnp.abs(forget_pre)))
+        carried = log_forget + stabilizer[:, h : h + 1]
+        state = jnp.maximum(carried, ingate_pre)
+        states = jnp.where(lane == h, state, states)
+        keep = jnp.broadcast_to(jnp.exp(carried - state), (rows, dim))
+        keeps[:, cut] = keep
+        write_key = jnp.exp(ingate_pre - state) * key
+        normal = keep * normalizer[:, h, :] + write_key
+        new_normalizer[:, h, :] = normal
+        denoms.append(jnp.sum(query * normal, axis=-1, keepdims=True))
+        turned[h, 0:rows, :] = query
+        turned[h, 16 : 16 + rows, :] = write_key
+        flipped[h] = turned[h].T
+    new_stabilizer[...] = states
+    copies = []
+    for t in range(rows):
+        for h in range(heads):
+            cut = slice(h * dim, (h + 1) * dim)
+            keep_row = keeps[t : t + 1, cut]
+            value_row = value[t : t + 1, cut]
+            total_row = jnp.zeros((8, dim), F32)
+            for low in range(0, dim, 8):
+                part = slice(low, low + 8)
+                block = keep_row * memory[t, h, part, :] + flipped[h, part, 16 + t : 17 + t] * value_row
+                fresh[t, h, part, :] = block
+                total_row = total_row + flipped[h, part, t : t + 1] * block
+            numer[t : t + 1, cut] = jnp.sum(total_row, axis=0, keepdims=True)
+        copies.append(pltpu.make_async_copy(fresh.at[t], new_memory.at[t], sems.at[t]))
+        copies[-1].start()
+    for h in range(heads):
+        cut = slice(h * dim, (h + 1) * dim)
+        outgate = rounded(total[:, 3 * width + h * dim : 3 * width + (h + 1) * dim])
+        hidden = numer[:, cut] / jnp.maximum(jnp.abs(denoms[h]), 1.0)
+        cell_out[:, cut] = (hidden / (1.0 + jnp.exp(-outgate))).astype(BF16)
+    for copy in copies:
+        copy.wait()
+
+
+def routing_kernel(group_width, rows_pad, index, weights, select, extra):
+    rows, chosen = index.shape
+    second = (index[:, 0:1] >= group_width).astype(F32)
+    row = lax.broadcasted_iota(jnp.int32, (rows, rows), 0)
+    col = lax.broadcasted_iota(jnp.int32, (rows, rows), 1)
+    earlier = (col < row).astype(F32)
+    before = jnp.dot(earlier, jnp.broadcast_to(second, (rows, LANES)), preferred_element_type=F32)
+    place = lax.broadcasted_iota(jnp.int32, (rows, LANES), 0).astype(F32)
+    slot = jnp.where(second > 0.5, rows_pad + before, place - before)
+    lane = lax.broadcasted_iota(jnp.int32, (rows, LANES), 1)
+    select[...] = (lane.astype(F32) == slot).astype(F32)
+    dense = jnp.zeros((rows, LANES), F32)
+    for k in range(chosen):
+        local = jnp.where(index[:, k : k + 1] >= group_width, index[:, k : k + 1] - group_width, index[:, k : k + 1])
+        hit = (lane == local) | (lane == local + group_width)
+        dense = dense + jnp.where(hit, weights[:, k : k + 1], 0.0)
+    high = rounded(dense)
+    extra[...] = jnp.where(lane < group_width, high, dense - high).astype(BF16)
+
+
+def mix_kernel(places, cell_out, tokens, gain, select, extra, *refs):
+    blocks, (resid, outgoing, mixed) = refs[: len(places)], refs[len(places) :]
+    width = tokens.shape[1]
+    me = lax.axis_index("ep")
+    piece = blocks[0].shape[2]
+    cell = cell_out[...]
+    for ref, bits_of in zip(blocks, places):
+        for number, bits in enumerate(bits_of):
+            block = jnp.dot(cell, ref[number], preferred_element_type=F32)
+            start = pl.multiple_of((me ^ bits) * piece, LANES)
+            mixed[:, pl.ds(start, piece)] = rounded(block)
+    total = tokens[...].astype(F32) + mixed[...]
+    resid[...] = total
+    scale = lax.rsqrt(jnp.mean(total * total, axis=-1, keepdims=True) + EPS)
+    moe_in = (total * scale * gain[...]).astype(BF16)
+    chips, rows_pad, _ = outgoing.shape
+    pick = select[:, : 2 * rows_pad].astype(BF16)
+    contract = (((0,), (0,)), ((), ()))
+    picked = lax.dot_general(pick, moe_in, contract, preferred_element_type=F32)
+    tail = lax.dot_general(pick, extra[...], contract, preferred_element_type=F32)
+    for group in range(2):
+        cut = slice(group * rows_pad, (group + 1) * rows_pad)
+        body = picked[cut].astype(BF16)
+        end = tail[cut].astype(BF16)
+        for c in range(chips // 2):
+            outgoing[group * (chips // 2) + c, :, :width] = body
+            outgoing[group * (chips // 2) + c, :, width:] = end
+
+
+def expert_kernel(group_width, direct, across, gate_weight, up_weight, down_weight, kept, sent):
+    width = gate_weight.shape[1]
+    half = direct.shape[0]
+    me = lax.axis_index("ep")
+    mine = me % group_width
+    x = jnp.concatenate((direct[:, :width], across[:, :width]), axis=0)
+    tail = jnp.concatenate((direct[:, width:], across[:, width:]), axis=0).astype(F32)
+    lane = lax.broadcasted_iota(jnp.int32, tail.shape, 1)
+    hit = (lane == mine) | (lane == mine + group_width)
+    weight = jnp.sum(jnp.where(hit, tail, 0.0), axis=1, keepdims=True)
+    gate = jnp.dot(x, gate_weight[0], preferred_element_type=F32)
+    upward = jnp.dot(x, up_weight[0], preferred_element_type=F32)
+    inner = (gate / (1.0 + jnp.exp(-gate)) * upward).astype(BF16)
+    step = 4 * LANES
+    for low in range(0, width, step):
+        out = jnp.dot(inner, down_weight[0, :, low : low + step], preferred_element_type=F32) * weight
+        kept[:, low : low + step] = out[:half]
+        sent[:, low : low + step] = out[half:].astype(BF16)
+
+
+def pair_kernel(kept, other, out):
+    out[...] = (kept[...] + other[...].astype(F32)).astype(BF16)
+
+
+def final_kernel(returned, select, resid, out):
+    chips, rows_pad, _ = returned.shape
+    sums = []
+    for group in range(2):
+        base = group * (chips // 2)
+        total = returned[base].astype(F32)
+        for c in range(1, chips // 2):
+            total = total + returned[base + c].astype(F32)
+        sums.append(total)
+    combined = jnp.concatenate(sums, axis=0)
+    picked = jnp.dot(
+        select[:, : 2 * rows_pad], combined,
+        preferred_element_type=F32, precision=lax.Precision.HIGHEST,
+    )
+    out[...] = (resid[...] + picked).astype(BF16)
+
+
+def on_device_fast(
+    tokens,
+    norm_gain,
+    query_weight,
+    key_weight,
+    value_weight,
+    outgate_weight,
+    ingate_weight,
+    forget_weight,
+    ingate_bias,
+    forget_bias,
+    memory,
+    normalizer,
+    stabilizer,
+    mixer_weight,
+    moe_gain,
+    expert_gate,
+    expert_up,
+    expert_down,
+    expert_index,
+    route_weights,
+):
+    ep_size = lax.axis_size("ep")
+    seq_count, model_width = tokens.shape
+    depth, cell_width = query_weight.shape
+    stations = ep_size // 4
+    chips = ep_size // 2
+    z_groups = [[k + 4 * z for z in range(stations)] for k in range(4)]
+    chip_groups = [[k + 2 * c for c in range(chips)] for k in range(2)]
+    expert_count = ep_size * expert_gate.shape[0]
+    group_width = expert_count // 2
+    chosen_k = expert_index.shape[1]
+    capacity = max(2, ((seq_count + 1) // 2 * chosen_k + group_width - 1) // group_width)
+    limit = min(seq_count, capacity * group_width // chosen_k)
+    rows = -(-limit // 8) * 8
+
+    pieces, bits_of = mixer_weight[None], [0]
+    batches = []
+    bit = 4
+    while bit < ep_size:
+        moved = swap(pieces, bit)
+        moved_bits = [b ^ bit for b in bits_of]
+        if 2 * bit < ep_size:
+            pieces = stack(pieces, moved)
+            bits_of = bits_of + moved_bits
+        else:
+            batches = [(pieces, bits_of), (moved, moved_bits)]
+        bit *= 2
+
+    wide = 4 * cell_width + LANES
+    joined, columns = local_call(
+        join_kernel,
+        [((depth, wide), BF16), ((stations, seq_count, model_width // stations), BF16)],
+        scratch=[
+            pltpu.VMEM((LANES, depth), F32),
+            pltpu.VMEM(tokens.shape, BF16),
+            pltpu.VMEM((2, ingate_weight.shape[1], depth), BF16),
+            pltpu.SemaphoreType.DMA((7,)),
+        ],
+        hbm=tuple(range(7)),
+        limit=60,
+        moved=2 * depth * wide * 2,
+    )(tokens, query_weight, key_weight, value_weight, outgate_weight, ingate_weight.T, forget_weight.T)
+    joined_y = swap(joined, 2)
+    joined_c = swap(joined, 1)
+    joined_yc = swap(joined_y, 1)
+    columns = lax.all_to_all(columns, "ep", 0, 0, tiled=True, axis_index_groups=z_groups)
+    (partial,) = local_call(
+        project_kernel,
+        [((stations, seq_count, wide), BF16)],
+        scratch=[
+            pltpu.VMEM((stations * seq_count, 4 * depth), F32),
+            pltpu.VMEM((4, depth, wide), BF16),
+            pltpu.VMEM((stations * seq_count, wide), F32),
+            pltpu.SemaphoreType.DMA((4,)),
+        ],
+        anywhere=(2, 3, 4, 5),
+        limit=60,
+        flops=2 * stations * seq_count * 4 * depth * wide,
+        moved=4 * depth * wide * 2,
+    )(columns, norm_gain[None], joined, joined_c, joined_y, joined_yc)
+    received = lax.all_to_all(partial, "ep", 0, 0, tiled=True, axis_index_groups=z_groups)
+    for batch, bits in list(batches):
+        batches.append((swap(batch, 2), [b ^ 2 for b in bits]))
+    for batch, bits in list(batches):
+        batches.append((swap(batch, 1), [b ^ 1 for b in bits]))
+    blocks = [batch for batch, _ in batches]
+    places = tuple(tuple(bits) for _, bits in batches)
+
+    select, extra = local_call(
+        functools.partial(routing_kernel, group_width, rows),
+        [((seq_count, LANES), F32), ((seq_count, LANES), BF16)],
+    )(expert_index, route_weights)
+
+    new_memory, new_normalizer, new_stabilizer, cell_out = local_call(
+        cell_kernel,
+        [
+            (memory.shape, F32),
+            (normalizer.shape, F32),
+            (stabilizer.shape, F32),
+            ((seq_count, cell_width), BF16),
+        ],
+        scratch=[
+            pltpu.VMEM(memory.shape[1:2] + (LANES, LANES), F32),
+            pltpu.VMEM(memory.shape[1:2] + (LANES, LANES), F32),
+            pltpu.VMEM((seq_count, cell_width), F32),
+            pltpu.VMEM((seq_count, cell_width), F32),
+            pltpu.VMEM(memory.shape, F32),
+            pltpu.SemaphoreType.DMA((seq_count,)),
+        ],
+        outs_hbm=(0,),
+        flops=6 * memory.size,
+        moved=8 * memory.size,
+        smem=(0, 1),
+        limit=16,
+    )(ingate_bias, forget_bias, received, tokens, memory, normalizer, stabilizer)
+
+    resid, outgoing = local_call(
+        functools.partial(mix_kernel, places),
+        [((seq_count, model_width), F32), ((chips, rows, model_width + LANES), BF16)],
+        scratch=[pltpu.VMEM((seq_count, model_width), F32)],
+        flops=2 * seq_count * cell_width * model_width,
+        moved=2 * cell_width * model_width,
+        limit=12,
+    )(cell_out, tokens, moe_gain[None], select, extra, *blocks)
+
+    direct = lax.all_to_all(outgoing, "ep", 0, 0, tiled=True, axis_index_groups=chip_groups)
+    direct = direct.reshape(chips * rows, model_width + LANES)
+    across = swap(direct, 1)
+    kept, sent = local_call(
+        functools.partial(expert_kernel, group_width),
+        [((chips * rows, model_width), F32), ((chips * rows, model_width), BF16)],
+        flops=6 * 2 * chips * rows * model_width * expert_gate.shape[2],
+        moved=6 * model_width * expert_gate.shape[2],
+        limit=24,
+    )(direct, across, expert_gate, expert_up, expert_down)
+    (summed,) = local_call(pair_kernel, [((chips * rows, model_width), BF16)])(kept, swap(sent, 1))
+    returned = lax.all_to_all(
+        summed.reshape(chips, rows, model_width), "ep", 0, 0, tiled=True, axis_index_groups=chip_groups
+    )
+    (layer_out,) = local_call(final_kernel, [((seq_count, model_width), BF16)])(returned, select, resid)
+    return (layer_out, new_memory, new_normalizer, new_stabilizer)
+
+
 def solution(mesh):
-    return jax.shard_map(
-        on_device,
-        mesh=mesh,
-        in_specs=(
-            P(("grp", "ep"), None),
-            P(),
-            P("ep", None),
-            P("ep", None),
-            P("ep", None),
-            P("ep", None),
-            P("ep", None),
-            P("ep", None),
-            P(),
-            P(),
-            P(("grp", "ep"), None, None, None),
-            P(("grp", "ep"), None, None),
-            P(("grp", "ep"), None),
-            P(None, "ep"),
-            P(),
-            P("ep", None, None),
-            P("ep", None, None),
-            P("ep", None, None),
-            P(("grp", "ep"), None),
-            P(("grp", "ep"), None),
-        ),
-        out_specs=(
-            P(("grp", "ep"), None),
-            P(("grp", "ep"), None, None, None),
-            P(("grp", "ep"), None, None),
-            P(("grp", "ep"), None),
-        ),
-        check_vma=False,
-    )
+    ep_size = mesh.shape["ep"]
+    aligned = ep_size % 8 == 0 and ep_size <= 16
+
+    def run(*arrays):
+        fits = aligned and arrays[13].shape[1] // ep_size % 128 == 0 and arrays[15].shape[0] == ep_size
+        fits = fits and arrays[2].shape[0] // ep_size % 128 == 0 and arrays[10].shape[2] == 128
+
+        def body(*blocks):
+            return (on_device_fast if fits else on_device_general)(*blocks)
+
+        step = jax.shard_map(
+            body, mesh=mesh, in_specs=ARG_SPECS, out_specs=OUT_SPECS, check_vma=False
+        )
+        return step(*arrays)
+
+    return run

time: 215 us -> 104 us (0.48)
  waiting for transfers between devices: 117 us -> 40.2 us
  Pallas kernels: 0 us -> 17.2 us
  blocking collectives: 36.9 us -> 22 us
  between operations: 15.1 us -> 0.87 us
  other arithmetic: 9.43 us -> 0 us
  matrix products: 9.42 us -> 0 us
  local copies, waits for them, and re-layouts: 11.4 us -> 4.1 us
  starting transfers between devices: 15.1 us -> 18.8 us
    unnamed x2 -> x0, waiting for transfers between devices: 92.5 us -> none
    ppermute x0 -> x13, waiting for transfers between devices: none -> 25.6 us  [swap(): return lax.ppermute(value, 'ep', [(i, i ^ bit) for i in range(size)])]
    all_gather x1 -> x0, blocking collectives: 20 us -> none  [on_device(): lax.all_gather(cell_out, 'ep', axis=0, tiled=True)]
    pallas_call x0 -> x9, Pallas kernels: none -> 17.2 us  [call(): pl.pallas_call(kernel, out_shape=[jax.ShapeDtypeStruct(*o) for o in outs]...]
    ppermute x0 -> x13, starting transfers between devices: none -> 11.9 us  [swap(): return lax.ppermute(value, 'ep', [(i, i ^ bit) for i in range(size)])]
    all_to_all x3 -> x2, waiting for transfers between devices: 24.3 us -> 14.7 us  [the longest x1 8.77 us: on_device_fast(): lax.all_to_all(summed.reshape(chips, rows, model_width), 'ep', 0, 0, tile...]
    dot_general x7 -> x0, matrix products: 9.42 us -> none  [the longest x1 2.56 us: on_device(): jnp.einsum('sxcf,xfd->sxcd', inner, expert_down, preferred_element_type=f32)]
    all_to_all x3 -> x2, starting transfers between devices: 15 us -> 6.87 us  [the longest x1 3.46 us: on_device_fast(): lax.all_to_all(partial, 'ep', 0, 0, tiled=True, axis_index_groups=z_groups)]
  transfers between devices with their start and end apart: 4 -> 15, of which waited for: 4 -> 6; matrix products, arithmetic and copies ran while one was open for 2% -> 2% of each run, Pallas kernels for 0% -> 10%
where the time goes in v1:
time: 104 us; the launch traced here: 103 us
  waiting for transfers between devices  40.2 us (39%)
  blocking collectives  22 us (21%)
  starting transfers between devices  18.8 us (18%)
  Pallas kernels  17.2 us (17%)
  local copies, waits for them, and re-layouts  4.1 us (4%)
    ppermute x13, waiting for transfers between devices, swap(): return lax.ppermute(value, 'ep', [(i, i ^ bit) for i in range(size)])  25.6 us
    pallas_call x9, Pallas kernels, call(): pl.pallas_call(kernel, out_shape=[jax.ShapeDtypeStruct(*o) for o in outs]...  17.2 us
    ppermute x13, starting transfers between devices, swap(): return lax.ppermute(value, 'ep', [(i, i ^ bit) for i in range(size)])  11.9 us
    all_to_all x1, blocking collectives, on_device_fast(): lax.all_to_all(outgoing, 'ep', 0, 0, tiled=True, axis_index_groups=chip_g...  11.4 us
    all_to_all x1, blocking collectives, on_device_fast(): lax.all_to_all(columns, 'ep', 0, 0, tiled=True, axis_index_groups=z_groups)  10.6 us
    all_to_all x1, waiting for transfers between devices, on_device_fast(): lax.all_to_all(summed.reshape(chips, rows, model_width), 'ep', 0, 0, tile...  8.77 us
    all_to_all x1, waiting for transfers between devices, on_device_fast(): lax.all_to_all(partial, 'ep', 0, 0, tiled=True, axis_index_groups=z_groups)  5.89 us
    unnamed x32, local copies, waits for them, and re-layouts  4.1 us
  transfers between devices with their start and end apart: 15, of which 6 were waited for; matrix products, arithmetic and copies ran while one was open for 2% of the time, Pallas kernels for 10%

profile of v1, /device:TPU:0, one launch (start us, length us, event | category | flops | bytes accessed | tf_op | source)
XLA Modules:
  0.0 103.2 jit_solution(17630643621334423689)
XLA Ops:
  0.7 2.2 %shard_map.219 = (bf16[128,2176]{1,0:T(8,128)(2,1)}, bf16[4,12,512]{2,1,0:T(8,128)(2,1)}) custom-call(bf16[12,2048]{1,0:T(8,128)(2,1)} %tokens.5, bf16[128,512]{1,0:T(8,128)(2,1)} %query.1, bf16[128,512]{1,0:T(8,128)(2,1)} %key.1, bf16[128,512]{1,0:T(8,128)(2,1)} %value.1, bf16[128,512]{1,0:T(8,128)(2,1)} %outgate.1, bf16[4,128]{1,0:T(4,128)(2,1)} %bitcast.13, ...), custom_call_target="tpu_custom_call" | custom-call | flops 1 | bytes 1114112 | tf_op jit(solution)/shard_map/pallas_call | solution.py:187
  2.9 3.1 %collective-permute-start.1 = (bf16[128,2176]{1,0:T(8,128)(2,1)}, bf16[128,2176]{1,0:T(8,128)(2,1)S(1)}, u32[]{:S(2)}, u32[]{:S(2)}) collective-permute-start(bf16[128,2176]{1,0:T(8,128)(2,1)} %get-tuple-element.17.own), channel_id=1, source_target_pairs={{0,2},{1,3},{2,0},{3,1},{4,6},{5,7},{6,4},{7,5},{8,10},{9,11},{10,... | collective-permute-start | bytes 1671176 | tf_op jit(solution)/shard_map/ppermute | solution.py:169
  5.9 1.6 %collective-permute-start.3 = (bf16[1,512,128]{2,1,0:T(8,128)(2,1)}, bf16[1,512,128]{2,1,0:T(8,128)(2,1)S(1)}, u32[]{:S(2)}, u32[]{:S(2)}) collective-permute-start(bf16[1,512,128]{2,1,0:T(8,128)(2,1)} %bitcast.10), channel_id=1, source_target_pairs={{0,4},{1,5},{2,6},{3,7},{4,0},{5,1},{6,2},{7,3},{8,12},{9,13},{10,... | collective-permute-start | bytes 393224 | tf_op jit(solution)/shard_map/ppermute | solution.py:169
  7.5 11.3 %collective-permute-done.1.side = bf16[128,2176]{1,0:T(8,128)(2,1)S(1)} collective-permute-done((bf16[128,2176]{1,0:T(8,128)(2,1)}, bf16[128,2176]{1,0:T(8,128)(2,1)S(1)}, u32[]{:S(2)}, u32[]{:S(2)}) %collective-permute-start.1) | collective-permute-done | bytes 557088 | tf_op jit(solution)/shard_map/ppermute | solution.py:169
  19.5 1.7 %shard_map.223.refs_0_ = bf16[2,512,128]{2,1,0:T(8,128)(2,1)} custom-call(bf16[1,512,128]{2,1,0:T(8,128)(2,1)} %bitcast.11, bf16[1,512,128]{2,1,0:T(8,128)(2,1)} %copy-done.11), custom_call_target="tpu_custom_call" | custom-call | flops 1 | bytes 524288 | tf_op jit(solution)/shard_map/pallas_call | solution.py:187
  21.2 2.9 %collective-permute-start.4 = (bf16[2,512,128]{2,1,0:T(8,128)(2,1)}, bf16[2,512,128]{2,1,0:T(8,128)(2,1)}, u32[]{:S(2)}, u32[]{:S(2)}) collective-permute-start(bf16[2,512,128]{2,1,0:T(8,128)(2,1)} %shard_map.223.refs_0_), channel_id=1, source_target_pairs={{0,8},{1,9},{2,10},{3,11},{4,12},{5,13},{6,14},{7,15},{8,0},{9,1},... | collective-permute-start | bytes 786440 | tf_op jit(solution)/shard_map/ppermute | solution.py:169
  24.1 1.5 %collective-permute-start.5 = (bf16[2,512,128]{2,1,0:T(8,128)(2,1)}, bf16[2,512,128]{2,1,0:T(8,128)(2,1)}, u32[]{:S(2)}, u32[]{:S(2)}) collective-permute-start(bf16[2,512,128]{2,1,0:T(8,128)(2,1)} %shard_map.223.refs_0_), channel_id=1, source_target_pairs={{0,2},{1,3},{2,0},{3,1},{4,6},{5,7},{6,4},{7,5},{8,10},{9,11},{10,... | collective-permute-start | bytes 786440 | tf_op jit(solution)/shard_map/ppermute | solution.py:169
  25.6 11.3 %collective-permute-done.4.refs_1_ = bf16[2,512,128]{2,1,0:T(8,128)(2,1)} collective-permute-done((bf16[2,512,128]{2,1,0:T(8,128)(2,1)}, bf16[2,512,128]{2,1,0:T(8,128)(2,1)}, u32[]{:S(2)}, u32[]{:S(2)}) %collective-permute-start.4) | collective-permute-done | bytes 262176 | tf_op jit(solution)/shard_map/ppermute | solution.py:169
  36.9 1.6 %collective-permute-start.6 = (bf16[2,512,128]{2,1,0:T(8,128)(2,1)}, bf16[2,512,128]{2,1,0:T(8,128)(2,1)}, u32[]{:S(2)}, u32[]{:S(2)}) collective-permute-start(bf16[2,512,128]{2,1,0:T(8,128)(2,1)} %collective-permute-done.4.refs_1_), channel_id=1, source_target_pairs={{0,2},{1,3},{2,0},{3,1},{4,6},{5,7},{6,4},{7,5},{8,10},{9,11},{10,... | collective-permute-start | bytes 786440 | tf_op jit(solution)/shard_map/ppermute | solution.py:169
  38.5 10.6 %all_to_all.20.columns = bf16[4,12,512]{2,1,0:T(8,128)(2,1)} all-to-all(bf16[4,12,512]{2,1,0:T(8,128)(2,1)} %get-tuple-element.16), channel_id=1, replica_groups={{0,4,8,12},{1,5,9,13},{2,6,10,14},{3,7,11,15},{16,20,24,28},{17,21,25,2..., dimensions={0} | all-to-all | bytes 98304 | tf_op jit(solution)/shard_map/all_to_all | solution.py:514
  49.1 3.4 %shard_map.220 = bf16[4,12,2176]{2,1,0:T(8,128)(2,1)} custom-call(bf16[4,12,512]{2,1,0:T(8,128)(2,1)} %all_to_all.20.columns, f32[1,2048]{1,0:T(1,128)} %bitcast.12, bf16[128,2176]{1,0:T(8,128)(2,1)} %get-tuple-element.17.own, bf16[128,2176]{1,0:T(8,128)(2,1)} %collective-permute-done.core, bf16[128,2176]{1,0:T(8,128)(2,1)} %copy-done.10, ...), custom_call_target="tpu_custom_call" | custom-call | flops 106954752 | bytes 2228224 | tf_op jit(solution)/shard_map/pallas_call | solution.py:187
  52.5 3.5 %all-to-all-start.1 = ((bf16[4,12,2176]{2,1,0:T(8,128)(2,1)}), bf16[4,12,2176]{2,1,0:T(8,128)(2,1)S(1)}, u32[]{:S(2)}, u32[]{:S(2)}) async-start(bf16[4,12,2176]{2,1,0:T(8,128)(2,1)} %shard_map.220), calls=%async_computation.1 | async-start | bytes 557056 | tf_op jit(solution)/shard_map/all_to_all | solution.py:529
  57.5 0.8 copy.24.stabilizer
  58.2 5.9 %all-to-all-done.1.received = bf16[4,12,2176]{2,1,0:T(8,128)(2,1)S(1)} async-done(((bf16[4,12,2176]{2,1,0:T(8,128)(2,1)}), bf16[4,12,2176]{2,1,0:T(8,128)(2,1)S(1)}, u32[]{:S(2)}, u32[]{:S(2)}) %all-to-all-start.1) | async-done | bytes 208928 | tf_op jit(solution)/shard_map/all_to_all | solution.py:529
  64.8 4.9 %shard_map.221 = (f32[12,4,128,128]{3,2,1,0:T(8,128)}, f32[12,4,128]{2,1,0:T(4,128)}, f32[12,4]{1,0:T(8,128)S(1)}, bf16[12,512]{1,0:T(8,128)(2,1)S(1)}) custom-call(f32[4]{0:T(128)S(1)} %copy-done.8, f32[4]{0:T(128)S(1)} %copy-done.9, bf16[4,12,2176]{2,1,0:T(8,128)(2,1)S(1)} %all-to-all-done.1.received, bf16[12,2048]{1,0:T(8,128)(2,1)S(1)} %copy-done.5, ...), custom_call_target="tpu_custom_call" | custom-call | flops 4718592 | bytes 6291456 | tf_op jit(solution)/shard_map/pallas_call | solution.py:187
  69.8 1.1 %copy-done.4 = bf16[2,512,128]{2,1,0:T(8,128)(2,1)S(1)} copy-done((bf16[2,512,128]{2,1,0:T(8,128)(2,1)S(1)}, bf16[2,512,128]{2,1,0:T(8,128)(2,1)}, u32[]{:S(2)}) %copy-start.4) | copy-done | bytes 262168
  70.9 2.1 %shard_map.224 = (f32[12,2048]{1,0:T(8,128)S(1)}, bf16[8,8,2176]{2,1,0:T(8,128)(2,1)S(1)}) custom-call(bf16[12,512]{1,0:T(8,128)(2,1)S(1)} %get-tuple-element.18.cell_out, bf16[12,2048]{1,0:T(8,128)(2,1)S(1)} %copy-done.5, f32[1,2048]{1,0:T(1,128)S(1)} %bitcast.9, f32[12,128]{1,0:T(8,128)S(1)} %get-tuple-element.19.select, ...), custom_call_target="tpu_custom_call" | custom-call | flops 25165824 | bytes 2097152 | tf_op jit(solution)/shard_map/pallas_call | solution.py:187
  73.0 11.4 %all_to_all.21 = bf16[8,8,2176]{2,1,0:T(8,128)(2,1)S(1)} all-to-all(bf16[8,8,2176]{2,1,0:T(8,128)(2,1)S(1)} %get-tuple-element.21), channel_id=1, replica_groups={{0,2,4,6,8,10,12,14},{1,3,5,7,9,11,13,15},{16,18,20,22,24,26,28,30},{17..., dimensions={0} | all-to-all | bytes 557056 | tf_op jit(solution)/shard_map/all_to_all | solution.py:574
  84.4 1.6 %collective-permute-done.11.across = bf16[64,2176]{1,0:T(8,128)(2,1)S(1)} collective-permute-done((bf16[64,2176]{1,0:T(8,128)(2,1)S(1)}, bf16[64,2176]{1,0:T(8,128)(2,1)S(1)}, u32[]{:S(2)}, u32[]{:S(2)}) %collective-permute-start.11) | collective-permute-done | bytes 278560 | tf_op jit(solution)/shard_map/ppermute | solution.py:169
  85.9 1.1 %shard_map.225 = (f32[64,2048]{1,0:T(8,128)S(1)}, bf16[64,2048]{1,0:T(8,128)(2,1)S(1)}) custom-call(bf16[64,2176]{1,0:T(8,128)(2,1)S(1)} %bitcast.8, bf16[64,2176]{1,0:T(8,128)(2,1)S(1)} %collective-permute-done.11.across, bf16[1,2048,512]{2,1,0:T(8,128)(2,1)S(1)} %copy-done.1, bf16[1,2048,512]{2,1,0:T(8,128)(2,1)S(1)} %copy-done.2, ...), custom_call_target="tpu_custom_call" | custom-call | flops 805306368 | bytes 6291456 | tf_op jit(solution)/shard_map/pallas_call | solution.py:187
  87.2 1.4 %collective-permute-done.12.other = bf16[64,2048]{1,0:T(8,128)(2,1)S(1)} collective-permute-done((bf16[64,2048]{1,0:T(8,128)(2,1)S(1)}, bf16[64,2048]{1,0:T(8,128)(2,1)S(1)}, u32[]{:S(2)}, u32[]{:S(2)}) %collective-permute-start.12) | collective-permute-done | bytes 262176 | tf_op jit(solution)/shard_map/ppermute | solution.py:169
  89.4 3.4 %all-to-all-start.3 = ((bf16[8,8,2048]{2,1,0:T(8,128)(2,1)}), bf16[8,8,2048]{2,1,0:T(8,128)(2,1)S(1)}, u32[]{:S(2)}, u32[]{:S(2)}) async-start(bf16[8,8,2048]{2,1,0:T(8,128)(2,1)} %bitcast.6), calls=%async_computation.3 | async-start | bytes 524288 | tf_op jit(solution)/shard_map/all_to_all | solution.py:585
  93.5 8.8 %all-to-all-done.3.returned = bf16[8,8,2048]{2,1,0:T(8,128)(2,1)S(1)} async-done(((bf16[8,8,2048]{2,1,0:T(8,128)(2,1)}), bf16[8,8,2048]{2,1,0:T(8,128)(2,1)S(1)}, u32[]{:S(2)}, u32[]{:S(2)}) %all-to-all-start.3) | async-done | bytes 262176 | tf_op jit(solution)/shard_map/all_to_all | solution.py:585
  102.2 0.9 shard_map.227
  (49 shorter events, 4.5 us)
Async XLA Ops:
  0.6 56.4 %copy-start.12 = (s32[12,6]{0,1:T(8,128)S(1)}, s32[12,6]{0,1:T(8,128)}, u32[]{:S(2)}) copy-start(s32[12,6]{0,1:T(8,128)} %param.38) | copy-start | bytes 868
  0.6 56.5 %copy-start.13 = (f32[12,6]{0,1:T(8,128)S(1)}, f32[12,6]{0,1:T(8,128)}, u32[]{:S(2)}) copy-start(f32[12,6]{0,1:T(8,128)} %param.39) | copy-start | bytes 868
  0.7 63.5 %copy-start = (f32[12,4,128,128]{3,2,1,0:T(8,128)S(1)}, f32[12,4,128,128]{3,2,1,0:T(8,128)}, u32[]{:S(2)}) copy-start(f32[12,4,128,128]{3,2,1,0:T(8,128)} %memory.1) | copy-start | bytes 9437188
  0.7 63.5 %copy-start.5 = (bf16[12,2048]{1,0:T(8,128)(2,1)S(1)}, bf16[12,2048]{1,0:T(8,128)(2,1)}, u32[]{:S(2)}) copy-start(bf16[12,2048]{1,0:T(8,128)(2,1)} %tokens.5) | copy-start | bytes 147460
  0.7 63.5 %copy-start.6 = (f32[12,4,128]{2,1,0:T(4,128)S(1)}, f32[12,4,128]{2,1,0:T(4,128)}, u32[]{:S(2)}) copy-start(f32[12,4,128]{2,1,0:T(4,128)} %normalizer.1) | copy-start | bytes 73732
  0.7 63.4 %copy-start.8 = (f32[4]{0:T(128)S(1)}, f32[4]{0:T(128)}, u32[]{:S(2)}) copy-start(f32[4]{0:T(128)} %ingate_bias.1) | copy-start | bytes 52
  2.9 15.9 %collective-permute-start.1 = (bf16[128,2176]{1,0:T(8,128)(2,1)}, bf16[128,2176]{1,0:T(8,128)(2,1)S(1)}, u32[]{:S(2)}, u32[]{:S(2)}) collective-permute-start(bf16[128,2176]{1,0:T(8,128)(2,1)} %get-tuple-element.17.own), channel_id=1, source_target_pairs={{0,2},{1,3},{2,0},{3,1},{4,6},{5,7},{6,4},{7,5},{8,10},{9,11},{10,... | collective-permute-start | bytes 1671176 | tf_op jit(solution)/shard_map/ppermute | solution.py:169
  5.9 12.8 %collective-permute-start.3 = (bf16[1,512,128]{2,1,0:T(8,128)(2,1)}, bf16[1,512,128]{2,1,0:T(8,128)(2,1)S(1)}, u32[]{:S(2)}, u32[]{:S(2)}) collective-permute-start(bf16[1,512,128]{2,1,0:T(8,128)(2,1)} %bitcast.10), channel_id=1, source_target_pairs={{0,4},{1,5},{2,6},{3,7},{4,0},{5,1},{6,2},{7,3},{8,12},{9,13},{10,... | collective-permute-start | bytes 393224 | tf_op jit(solution)/shard_map/ppermute | solution.py:169
  7.5 41.6 %collective-permute-start = (bf16[128,2176]{1,0:T(8,128)(2,1)}, bf16[128,2176]{1,0:T(8,128)(2,1)}, u32[]{:S(2)}, u32[]{:S(2)}) collective-permute-start(bf16[128,2176]{1,0:T(8,128)(2,1)} %get-tuple-element.17.own), channel_id=1, source_target_pairs={{0,1},{1,0},{2,3},{3,2},{4,5},{5,4},{6,7},{7,6},{8,9},{9,8},{10,11... | collective-permute-start | bytes 1671176 | tf_op jit(solution)/shard_map/ppermute | solution.py:169
  18.8 30.3 %copy-start.10 = (bf16[128,2176]{1,0:T(8,128)(2,1)}, bf16[128,2176]{1,0:T(8,128)(2,1)S(1)}, u32[]{:S(2)}) copy-start(bf16[128,2176]{1,0:T(8,128)(2,1)S(1)} %collective-permute-done.1.side) | copy-start | bytes 1671172
  18.8 30.3 %collective-permute-start.2 = (bf16[128,2176]{1,0:T(8,128)(2,1)S(1)}, bf16[128,2176]{1,0:T(8,128)(2,1)}, u32[]{:S(2)}, u32[]{:S(2)}) collective-permute-start(bf16[128,2176]{1,0:T(8,128)(2,1)S(1)} %collective-permute-done.1.side), channel_id=1, source_target_pairs={{0,1},{1,0},{2,3},{3,2},{4,5},{5,4},{6,7},{7,6},{8,9},{9,8},{10,11... | collective-permute-start | bytes 1671176 | tf_op jit(solution)/shard_map/ppermute | solution.py:169
  21.2 15.7 %collective-permute-start.4 = (bf16[2,512,128]{2,1,0:T(8,128)(2,1)}, bf16[2,512,128]{2,1,0:T(8,128)(2,1)}, u32[]{:S(2)}, u32[]{:S(2)}) collective-permute-start(bf16[2,512,128]{2,1,0:T(8,128)(2,1)} %shard_map.223.refs_0_), channel_id=1, source_target_pairs={{0,8},{1,9},{2,10},{3,11},{4,12},{5,13},{6,14},{7,15},{8,0},{9,1},... | collective-permute-start | bytes 786440 | tf_op jit(solution)/shard_map/ppermute | solution.py:169
  24.1 32.5 %collective-permute-start.5 = (bf16[2,512,128]{2,1,0:T(8,128)(2,1)}, bf16[2,512,128]{2,1,0:T(8,128)(2,1)}, u32[]{:S(2)}, u32[]{:S(2)}) collective-permute-start(bf16[2,512,128]{2,1,0:T(8,128)(2,1)} %shard_map.223.refs_0_), channel_id=1, source_target_pairs={{0,2},{1,3},{2,0},{3,1},{4,6},{5,7},{6,4},{7,5},{8,10},{9,11},{10,... | collective-permute-start | bytes 786440 | tf_op jit(solution)/shard_map/ppermute | solution.py:169
  36.9 19.7 %collective-permute-start.6 = (bf16[2,512,128]{2,1,0:T(8,128)(2,1)}, bf16[2,512,128]{2,1,0:T(8,128)(2,1)}, u32[]{:S(2)}, u32[]{:S(2)}) collective-permute-start(bf16[2,512,128]{2,1,0:T(8,128)(2,1)} %collective-permute-done.4.refs_1_), channel_id=1, source_target_pairs={{0,2},{1,3},{2,0},{3,1},{4,6},{5,7},{6,4},{7,5},{8,10},{9,11},{10,... | collective-permute-start | bytes 786440 | tf_op jit(solution)/shard_map/ppermute | solution.py:169
  52.5 11.6 %all-to-all-start.1 = ((bf16[4,12,2176]{2,1,0:T(8,128)(2,1)}), bf16[4,12,2176]{2,1,0:T(8,128)(2,1)S(1)}, u32[]{:S(2)}, u32[]{:S(2)}) async-start(bf16[4,12,2176]{2,1,0:T(8,128)(2,1)} %shard_map.220), calls=%async_computation.1 | async-start | bytes 557056 | tf_op jit(solution)/shard_map/all_to_all | solution.py:529
  56.0 13.8 %collective-permute-start.7 = (bf16[2,512,128]{2,1,0:T(8,128)(2,1)}, bf16[2,512,128]{2,1,0:T(8,128)(2,1)}, u32[]{:S(2)}, u32[]{:S(2)}) collective-permute-start(bf16[2,512,128]{2,1,0:T(8,128)(2,1)} %shard_map.223.refs_0_), channel_id=1, source_target_pairs={{0,1},{1,0},{2,3},{3,2},{4,5},{5,4},{6,7},{7,6},{8,9},{9,8},{10,11... | collective-permute-start | bytes 786440 | tf_op jit(solution)/shard_map/ppermute | solution.py:169
  56.1 13.7 %collective-permute-start.8 = (bf16[2,512,128]{2,1,0:T(8,128)(2,1)}, bf16[2,512,128]{2,1,0:T(8,128)(2,1)}, u32[]{:S(2)}, u32[]{:S(2)}) collective-permute-start(bf16[2,512,128]{2,1,0:T(8,128)(2,1)} %collective-permute-done.4.refs_1_), channel_id=1, source_target_pairs={{0,1},{1,0},{2,3},{3,2},{4,5},{5,4},{6,7},{7,6},{8,9},{9,8},{10,11... | collective-permute-start | bytes 786440 | tf_op jit(solution)/shard_map/ppermute | solution.py:169
  56.6 13.2 %collective-permute-start.9 = (bf16[2,512,128]{2,1,0:T(8,128)(2,1)}, bf16[2,512,128]{2,1,0:T(8,128)(2,1)}, u32[]{:S(2)}, u32[]{:S(2)}) collective-permute-start(bf16[2,512,128]{2,1,0:T(8,128)(2,1)} %collective-permute-done.5.refs_2_), channel_id=1, source_target_pairs={{0,1},{1,0},{2,3},{3,2},{4,5},{5,4},{6,7},{7,6},{8,9},{9,8},{10,11... | collective-permute-start | bytes 786440 | tf_op jit(solution)/shard_map/ppermute | solution.py:169
  56.6 13.1 %collective-permute-start.10 = (bf16[2,512,128]{2,1,0:T(8,128)(2,1)}, bf16[2,512,128]{2,1,0:T(8,128)(2,1)}, u32[]{:S(2)}, u32[]{:S(2)}) collective-permute-start(bf16[2,512,128]{2,1,0:T(8,128)(2,1)} %collective-permute-done.6.refs_3_), channel_id=1, source_target_pairs={{0,1},{1,0},{2,3},{3,2},{4,5},{5,4},{6,7},{7,6},{8,9},{9,8},{10,11... | collective-permute-start | bytes 786440 | tf_op jit(solution)/shard_map/ppermute | solution.py:169
  64.8 21.1 %copy-start.2 = (bf16[1,2048,512]{2,1,0:T(8,128)(2,1)S(1)}, bf16[1,2048,512]{2,1,0:T(8,128)(2,1)}, u32[]{:S(2)}) copy-start(bf16[1,2048,512]{2,1,0:T(8,128)(2,1)} %up_weight.1) | copy-start | bytes 6291460
  64.8 21.1 %copy-start.3 = (bf16[1,512,2048]{2,1,0:T(8,128)(2,1)S(1)}, bf16[1,512,2048]{2,1,0:T(8,128)(2,1)}, u32[]{:S(2)}) copy-start(bf16[1,512,2048]{2,1,0:T(8,128)(2,1)} %down_weight.1) | copy-start | bytes 6291460
  84.4 1.6 %collective-permute-start.11 = (bf16[64,2176]{1,0:T(8,128)(2,1)S(1)}, bf16[64,2176]{1,0:T(8,128)(2,1)S(1)}, u32[]{:S(2)}, u32[]{:S(2)}) collective-permute-start(bf16[64,2176]{1,0:T(8,128)(2,1)S(1)} %bitcast.7), channel_id=1, source_target_pairs={{0,1},{1,0},{2,3},{3,2},{4,5},{5,4},{6,7},{7,6},{8,9},{9,8},{10,11... | collective-permute-start | bytes 835592 | tf_op jit(solution)/shard_map/ppermute | solution.py:169
  87.0 1.6 %collective-permute-start.12 = (bf16[64,2048]{1,0:T(8,128)(2,1)S(1)}, bf16[64,2048]{1,0:T(8,128)(2,1)S(1)}, u32[]{:S(2)}, u32[]{:S(2)}) collective-permute-start(bf16[64,2048]{1,0:T(8,128)(2,1)S(1)} %get-tuple-element.23), channel_id=1, source_target_pairs={{0,1},{1,0},{2,3},{3,2},{4,5},{5,4},{6,7},{7,6},{8,9},{9,8},{10,11... | collective-permute-start | bytes 786440 | tf_op jit(solution)/shard_map/ppermute | solution.py:169
  89.4 12.9 %all-to-all-start.3 = ((bf16[8,8,2048]{2,1,0:T(8,128)(2,1)}), bf16[8,8,2048]{2,1,0:T(8,128)(2,1)S(1)}, u32[]{:S(2)}, u32[]{:S(2)}) async-start(bf16[8,8,2048]{2,1,0:T(8,128)(2,1)} %bitcast.6), calls=%async_computation.3 | async-start | bytes 524288 | tf_op jit(solution)/shard_map/all_to_all | solution.py:585
  (5 other events, 35.9 us)

commit v2 on v1

--- a/solution.py
+++ b/solution.py
@@ -193,7 +193,7 @@
                 for i in range(len(outs))
             ],
             scratch_shapes=list(scratch),
-            compiler_params=pltpu.CompilerParams(vmem_limit_bytes=limit * 2**20),
+            compiler_params=pltpu.CompilerParams(vmem_limit_bytes=int(limit * 2**20)),
             cost_estimate=pl.CostEstimate(
                 flops=flops, bytes_accessed=moved, transcendentals=0
             ),
@@ -255,36 +255,31 @@
         copy.wait()
 
 
-def project_kernel(columns, gain, own, core, side, cross, out, scaled, weights, total, sems):
+def project_kernel(bits_of, columns, gain, first, second, *refs):
+    before, out, scaled = refs if len(refs) == 3 else (None,) + refs
     stations, rows, part = columns.shape
-    depth = own.shape[0]
-    copies = [
-        pltpu.make_async_copy(ref, weights.at[i], sems.at[i])
-        for i, ref in enumerate((own, core, side, cross))
-    ]
-    for copy in copies:
-        copy.start()
+    depth = first.shape[0]
     me = lax.axis_index("ep")
     station, place = me // 4, me % 4
     gain_here = gain[:, pl.ds(pl.multiple_of(station * part, LANES), part)]
     for z in range(stations):
         scaled[z * rows : (z + 1) * rows, :] = columns[z].astype(F32) * gain_here
-    width = out.shape[2]
+    parts = []
+    for bits in bits_of:
+        start = pl.multiple_of((place ^ bits) * depth, LANES)
+        parts.append(scaled[:, pl.ds(start, depth)].astype(BF16))
+    width = out.shape[-1]
     step = 4 * LANES
-    for bits, copy in enumerate(copies):
-        start = pl.multiple_of((place ^ bits) * depth, LANES)
-        part_x = scaled[:, pl.ds(start, depth)].astype(BF16)
-        copy.wait()
-        for low in range(0, width, step):
-            high = min(low + step, width)
-            term = jnp.dot(part_x, weights[bits, :, low:high], preferred_element_type=F32)
-            if bits:
-                term = term + total[:, low:high]
-            if bits < 3:
-                total[:, low:high] = term
-            else:
-                for z in range(stations):
-                    out[z, :, low:high] = term[z * rows : (z + 1) * rows].astype(BF16)
+    for low in range(0, width, step):
+        high = min(low + step, width)
+        term = jnp.dot(parts[0], first[:, low:high], preferred_element_type=F32)
+        term = term + jnp.dot(parts[1], second[:, low:high], preferred_element_type=F32)
+        if before is None:
+            out[:, low:high] = term
+            continue
+        term = term + before[:, low:high]
+        for z in range(stations):
+            out[z, :, low:high] = term[z * rows : (z + 1) * rows].astype(BF16)
 
 
 def rounded(value):
@@ -292,16 +287,17 @@
 
 
 def cell_kernel(
-    ingate_bias, forget_bias, received, tokens, memory, normalizer, stabilizer,
-    new_memory, new_normalizer, new_stabilizer, cell_out,
-    turned, flipped, keeps, numer, fresh, sems,
+    received, memory, side, new_memory, new_normalizer, new_stabilizer, cell_out,
+    turned, flipped, spread, keeps, numer, fresh, sems,
 ):
     stations, rows, _ = received.shape
     heads = memory.shape[1]
     dim = memory.shape[2]
     width = heads * dim
-    stream = tokens[...].astype(F32)
-    scale = lax.rsqrt(jnp.mean(stream * stream, axis=-1, keepdims=True) + EPS)
+    low = side.shape[1] - 4 * LANES
+    model_width = (low - width) // 2
+    scale = side[:, low : low + 1]
+    known = side[:, low + 2 * LANES : low + 3 * LANES]
     total = received[0].astype(F32)
     for z in range(1, stations):
         total = total + received[z].astype(F32)
@@ -311,39 +307,47 @@
     lane = lax.broadcasted_iota(jnp.int32, (rows, heads), 1)
     states = jnp.zeros((rows, heads), F32)
     denoms = []
+    turned[...] = jnp.zeros_like(turned)
+    spread[...] = jnp.zeros_like(spread)
+    spread[:, 0:16, 0:dim] = jnp.ones((heads, 16, dim), F32)
     for h in range(heads):
         cut = slice(h * dim, (h + 1) * dim)
         query = rounded(total[:, h * dim : (h + 1) * dim])
         key = rounded(total[:, width + h * dim : width + (h + 1) * dim]) * dim ** (-0.5)
-        ingate_pre = gates[:, h : h + 1] + ingate_bias[h]
-        forget_pre = gates[:, heads + h : heads + h + 1] + forget_bias[h]
+        ingate_pre = gates[:, h : h + 1] + known[:, 40 + h : 41 + h]
+        forget_pre = gates[:, heads + h : heads + h + 1] + known[:, 48 + h : 49 + h]
         log_forget = jnp.minimum(forget_pre, 0.0) - jnp.log1p(jnp.exp(-jnp.abs(forget_pre)))
-        carried = log_forget + stabilizer[:, h : h + 1]
+        carried = log_forget + known[:, 32 + h : 33 + h]
         state = jnp.maximum(carried, ingate_pre)
         states = jnp.where(lane == h, state, states)
         keep = jnp.broadcast_to(jnp.exp(carried - state), (rows, dim))
         keeps[:, cut] = keep
         write_key = jnp.exp(ingate_pre - state) * key
-        normal = keep * normalizer[:, h, :] + write_key
+        base = 2 * model_width + h * dim
+        normal = keep * side[:, base : base + dim] + write_key
         new_normalizer[:, h, :] = normal
         denoms.append(jnp.sum(query * normal, axis=-1, keepdims=True))
+        high = rounded(write_key)
+        middle = rounded(write_key - high)
         turned[h, 0:rows, :] = query
-        turned[h, 16 : 16 + rows, :] = write_key
-        flipped[h] = turned[h].T
+        turned[h, 16 : 16 + rows, :] = high
+        turned[h, 32 : 32 + rows, :] = middle
+        turned[h, 48 : 48 + rows, :] = rounded(write_key - high - middle)
+        flipped[h] = turned[h].T.astype(BF16)
+        for i in range(1, 4):
+            spread[h, 16 * i : 16 * i + rows, dim:] = value[:, cut]
     new_stabilizer[...] = states
     copies = []
+    which = lax.broadcasted_iota(jnp.int32, (64, 2 * dim), 0) % 16
+    spreads = [spread[h].astype(BF16) for h in range(heads)]
     for t in range(rows):
         for h in range(heads):
             cut = slice(h * dim, (h + 1) * dim)
-            keep_row = keeps[t : t + 1, cut]
-            value_row = value[t : t + 1, cut]
-            total_row = jnp.zeros((8, dim), F32)
-            for low in range(0, dim, 8):
-                part = slice(low, low + 8)
-                block = keep_row * memory[t, h, part, :] + flipped[h, part, 16 + t : 17 + t] * value_row
-                fresh[t, h, part, :] = block
-                total_row = total_row + flipped[h, part, t : t + 1] * block
-            numer[t : t + 1, cut] = jnp.sum(total_row, axis=0, keepdims=True)
+            row_only = jnp.where(which == t, spreads[h], jnp.zeros_like(spreads[h]))
+            both = jnp.dot(flipped[h][:, :64], row_only, preferred_element_type=F32)
+            block = keeps[t : t + 1, cut] * memory[t, h] + both[:, dim:]
+            fresh[t, h] = block
+            numer[t : t + 1, cut] = jnp.sum(both[:, :dim] * block, axis=0, keepdims=True)
         copies.append(pltpu.make_async_copy(fresh.at[t], new_memory.at[t], sems.at[t]))
         copies[-1].start()
     for h in range(heads):
@@ -355,81 +359,172 @@
         copy.wait()
 
 
-def routing_kernel(group_width, rows_pad, index, weights, select, extra):
-    rows, chosen = index.shape
-    second = (index[:, 0:1] >= group_width).astype(F32)
+def mix_kernel(places, cell_out, side, *refs):
+    blocks, (resid, outgoing, mixed) = refs[: len(places)], refs[len(places) :]
+    cell = cell_out[...]
+    model_width = resid.shape[1]
+    low = side.shape[1] - 4 * LANES
+    select = side[:, low + LANES : low + 2 * LANES]
+    extra = side[:, low + 3 * LANES : low + 4 * LANES].astype(BF16)
+    me = lax.axis_index("ep")
+    piece = blocks[0].shape[2]
+    for i, bits_of in enumerate(places):
+        for number, bits in enumerate(bits_of):
+            block = jnp.dot(cell, blocks[i][number], preferred_element_type=F32)
+            start = pl.multiple_of((me ^ bits) * piece, LANES)
+            mixed[:, pl.ds(start, piece)] = rounded(block)
+    level = side[:, 0:model_width] + mixed[...]
+    resid[...] = level
+    scale = lax.rsqrt(jnp.mean(level * level, axis=-1, keepdims=True) + EPS)
+    moe_in = (level * scale * side[:, model_width : 2 * model_width]).astype(BF16)
+    chips, rows_pad, packed = outgoing.shape
+    main = packed - LANES
+    tail = moe_in.shape[1] - main
+    contract = (((0,), (0,)), ((), ()))
+
+    def gathered(number, values):
+        pick = select[:, number * 2 * rows_pad : (number + 1) * 2 * rows_pad].astype(BF16)
+        return lax.dot_general(pick, values, contract, preferred_element_type=F32)
+
+    parts = []
+    if tail:
+        for j in range(main // tail):
+            parts.append(gathered(0, moe_in[:, j * tail : (j + 1) * tail]) + gathered(1 + j, moe_in[:, main:]))
+    else:
+        parts.append(gathered(0, moe_in))
+    parts.append(gathered(0, extra))
+    low = 0
+    for value in parts:
+        high = low + value.shape[1]
+        for group in range(2):
+            body = value[group * rows_pad : (group + 1) * rows_pad].astype(BF16)
+            for c in range(chips // 2):
+                outgoing[group * (chips // 2) + c, :, low:high] = body
+        low = high
+
+
+def routing_kernel(
+    group_width, limit, rows_pad, tails,
+    ingate_bias, forget_bias, index, weights, tokens, gain, normalizer, stabilizer,
+    select, side, small,
+):
+    chosen, rows = index.shape
+    heads, dim = normalizer.shape[1:]
+    width = tokens.shape[1]
+    stream = tokens[...].astype(F32)
+    scale = lax.rsqrt(jnp.mean(stream * stream, axis=-1, keepdims=True) + EPS)
+    side[:, 0:width] = stream
+    side[:, width : 2 * width] = jnp.broadcast_to(gain[...], (rows, width))
+    low = 2 * width
+    for h in range(heads):
+        side[:, low : low + dim] = normalizer[:, h, :]
+        low += dim
+    side[:, low : low + LANES] = jnp.broadcast_to(scale, (rows, LANES))
+    small[...] = jnp.zeros_like(small)
+    small[0:chosen, 0:rows] = index[...].astype(F32)
+    small[64 : 64 + chosen, 0:rows] = weights[...]
+    small[32 : 32 + heads, 0:rows] = stabilizer[...]
+    for h in range(heads):
+        small[40 + h : 41 + h, :] = jnp.full((1, LANES), ingate_bias[h], F32)
+        small[48 + h : 49 + h, :] = jnp.full((1, LANES), forget_bias[h], F32)
+    flat = small[...].T
+    experts = flat[0:rows, :]
+    second = (experts[:, 0:1] >= group_width).astype(F32)
     row = lax.broadcasted_iota(jnp.int32, (rows, rows), 0)
     col = lax.broadcasted_iota(jnp.int32, (rows, rows), 1)
     earlier = (col < row).astype(F32)
     before = jnp.dot(earlier, jnp.broadcast_to(second, (rows, LANES)), preferred_element_type=F32)
     place = lax.broadcasted_iota(jnp.int32, (rows, LANES), 0).astype(F32)
-    slot = jnp.where(second > 0.5, rows_pad + before, place - before)
-    lane = lax.broadcasted_iota(jnp.int32, (rows, LANES), 1)
-    select[...] = (lane.astype(F32) == slot).astype(F32)
+    rank = jnp.where(second > 0.5, before, place - before)
+    lane = lax.broadcasted_iota(jnp.int32, (rows, LANES), 1).astype(F32)
+    base = jnp.where(second > 0.5, float(rows_pad), 0.0)
+    chosen_lanes = lane == base + rank
+    if tails:
+        turn = jnp.zeros_like(rank)
+        for q in range(1, limit // tails):
+            turn = turn + (rank >= q * tails).astype(F32)
+        within = rank - turn * tails
+        chosen_lanes = chosen_lanes | (
+            lane == (1.0 + within) * (2 * rows_pad) + base + limit + turn
+        )
+    select[...] = chosen_lanes.astype(F32)
+    side[:, low + LANES : low + 2 * LANES] = chosen_lanes.astype(F32)
+    side[:, low + 2 * LANES : low + 3 * LANES] = flat[0:rows, :]
     dense = jnp.zeros((rows, LANES), F32)
     for k in range(chosen):
-        local = jnp.where(index[:, k : k + 1] >= group_width, index[:, k : k + 1] - group_width, index[:, k : k + 1])
+        expert = experts[:, k : k + 1]
+        local = jnp.where(expert >= group_width, expert - group_width, expert)
         hit = (lane == local) | (lane == local + group_width)
-        dense = dense + jnp.where(hit, weights[:, k : k + 1], 0.0)
+        dense = dense + jnp.where(hit, flat[0:rows, 64 + k : 65 + k], 0.0)
     high = rounded(dense)
-    extra[...] = jnp.where(lane < group_width, high, dense - high).astype(BF16)
-
-
-def mix_kernel(places, cell_out, tokens, gain, select, extra, *refs):
-    blocks, (resid, outgoing, mixed) = refs[: len(places)], refs[len(places) :]
-    width = tokens.shape[1]
+    side[:, low + 3 * LANES : low + 4 * LANES] = jnp.where(lane < group_width, high, dense - high)
+
+
+def sorted_rows(count, rows_pad, limit, tails, j, back):
+    row = lax.broadcasted_iota(jnp.int32, (count, count), 0)
+    col = lax.broadcasted_iota(jnp.int32, (count, count), 1)
+    spare, real = (row, col) if back else (col, row)
+    same = (spare // rows_pad) == (real // rows_pad)
+    spare, real = spare % rows_pad, real % rows_pad
+    hit = same & (spare >= limit) & (real == (spare - limit) * tails + j) & (real < limit)
+    return jnp.where(hit, 1.0, 0.0).astype(BF16)
+
+
+def expert_kernel(
+    group_width, rows_pad, limit, tails, rows_in,
+    gate0, up0, down0, gate1, up1, down1, out,
+):
+    count = rows_in.shape[0]
+    main = out.shape[1]
+    width = gate0.shape[1]
+    tail = width - main
     me = lax.axis_index("ep")
-    piece = blocks[0].shape[2]
-    cell = cell_out[...]
-    for ref, bits_of in zip(blocks, places):
-        for number, bits in enumerate(bits_of):
-            block = jnp.dot(cell, ref[number], preferred_element_type=F32)
-            start = pl.multiple_of((me ^ bits) * piece, LANES)
-            mixed[:, pl.ds(start, piece)] = rounded(block)
-    total = tokens[...].astype(F32) + mixed[...]
-    resid[...] = total
-    scale = lax.rsqrt(jnp.mean(total * total, axis=-1, keepdims=True) + EPS)
-    moe_in = (total * scale * gain[...]).astype(BF16)
-    chips, rows_pad, _ = outgoing.shape
-    pick = select[:, : 2 * rows_pad].astype(BF16)
-    contract = (((0,), (0,)), ((), ()))
-    picked = lax.dot_general(pick, moe_in, contract, preferred_element_type=F32)
-    tail = lax.dot_general(pick, extra[...], contract, preferred_element_type=F32)
-    for group in range(2):
-        cut = slice(group * rows_pad, (group + 1) * rows_pad)
-        body = picked[cut].astype(BF16)
-        end = tail[cut].astype(BF16)
-        for c in range(chips // 2):
-            outgoing[group * (chips // 2) + c, :, :width] = body
-            outgoing[group * (chips // 2) + c, :, width:] = end
-
-
-def expert_kernel(group_width, direct, across, gate_weight, up_weight, down_weight, kept, sent):
-    width = gate_weight.shape[1]
-    half = direct.shape[0]
-    me = lax.axis_index("ep")
-    mine = me % group_width
-    x = jnp.concatenate((direct[:, :width], across[:, :width]), axis=0)
-    tail = jnp.concatenate((direct[:, width:], across[:, width:]), axis=0).astype(F32)
-    lane = lax.broadcasted_iota(jnp.int32, tail.shape, 1)
-    hit = (lane == mine) | (lane == mine + group_width)
-    weight = jnp.sum(jnp.where(hit, tail, 0.0), axis=1, keepdims=True)
-    gate = jnp.dot(x, gate_weight[0], preferred_element_type=F32)
-    upward = jnp.dot(x, up_weight[0], preferred_element_type=F32)
-    inner = (gate / (1.0 + jnp.exp(-gate)) * upward).astype(BF16)
-    step = 4 * LANES
-    for low in range(0, width, step):
-        out = jnp.dot(inner, down_weight[0, :, low : low + step], preferred_element_type=F32) * weight
-        kept[:, low : low + step] = out[:half]
-        sent[:, low : low + step] = out[half:].astype(BF16)
-
-
-def pair_kernel(kept, other, out):
-    out[...] = (kept[...] + other[...].astype(F32)).astype(BF16)
-
-
-def final_kernel(returned, select, resid, out):
-    chips, rows_pad, _ = returned.shape
+    x = rows_in[:, :main]
+    if tail:
+        end = None
+        for j in range(tails):
+            move = sorted_rows(count, rows_pad, limit, tails, j, False)
+            term = jnp.dot(move, rows_in[:, j * tail : (j + 1) * tail], preferred_element_type=F32)
+            end = term if end is None else end + term
+        x = jnp.concatenate((x, end.astype(BF16)), axis=1)
+    info = rows_in[:, main:].astype(F32)
+    lane = lax.broadcasted_iota(jnp.int32, info.shape, 1)
+    inners = []
+    weights = []
+    for bit, (gate_weight, up_weight) in enumerate(((gate0, up0), (gate1, up1))):
+        mine = (me ^ bit) % group_width
+        hit = (lane == mine) | (lane == mine + group_width)
+        weights.append(jnp.sum(jnp.where(hit, info, 0.0), axis=1, keepdims=True))
+        gate = jnp.dot(x, gate_weight[0], preferred_element_type=F32)
+        upward = jnp.dot(x, up_weight[0], preferred_element_type=F32)
+        inners.append((gate / (1.0 + jnp.exp(-gate)) * upward).astype(BF16))
+
+    def result(low, high):
+        total = 0.0
+        for inner, down, weight in zip(inners, (down0, down1), weights):
+            total = total + weight * jnp.dot(inner, down[0, :, low:high], preferred_element_type=F32)
+        return total.astype(BF16)
+
+    if not tail:
+        step = 4 * LANES
+        for low in range(0, width, step):
+            out[:, low : low + step] = result(low, low + step)
+        return
+    end = result(main, width)
+    place = lax.broadcasted_iota(jnp.int32, (count, tail), 0) % rows_pad
+    for j in range(tails):
+        low, high = j * tail, (j + 1) * tail
+        move = sorted_rows(count, rows_pad, limit, tails, j, True)
+        moved = jnp.dot(move, end, preferred_element_type=F32)
+        body = result(low, high).astype(F32)
+        out[:, low:high] = jnp.where(place < limit, body, moved).astype(BF16)
+
+
+def final_kernel(tails, returned, select, resid_far, out, resid, sem):
+    chips, rows_pad, main = returned.shape
+    copy = pltpu.make_async_copy(resid_far, resid, sem)
+    copy.start()
+    tail = out.shape[1] - main
     sums = []
     for group in range(2):
         base = group * (chips // 2)
@@ -438,11 +533,22 @@
             total = total + returned[base + c].astype(F32)
         sums.append(total)
     combined = jnp.concatenate(sums, axis=0)
-    picked = jnp.dot(
-        select[:, : 2 * rows_pad], combined,
-        preferred_element_type=F32, precision=lax.Precision.HIGHEST,
-    )
-    out[...] = (resid[...] + picked).astype(BF16)
+    high = combined.astype(BF16)
+    low = (combined - high.astype(F32)).astype(BF16)
+
+    def picked(number, cut):
+        pick = select[:, number * 2 * rows_pad : (number + 1) * 2 * rows_pad].astype(BF16)
+        return jnp.dot(pick, high[:, cut], preferred_element_type=F32) + jnp.dot(
+            pick, low[:, cut], preferred_element_type=F32
+        )
+
+    copy.wait()
+    out[:, :main] = (resid[:, :main] + picked(0, slice(0, main))).astype(BF16)
+    if tail:
+        end = resid[:, main:]
+        for j in range(tails):
+            end = end + picked(1 + j, slice(j * tail, (j + 1) * tail))
+        out[:, main:] = end.astype(BF16)
 
 
 def on_device_fast(
@@ -480,6 +586,13 @@
     capacity = max(2, ((seq_count + 1) // 2 * chosen_k + group_width - 1) // group_width)
     limit = min(seq_count, capacity * group_width // chosen_k)
     rows = -(-limit // 8) * 8
+    spare = rows - limit
+    tails = limit // spare if spare and limit % spare == 0 else 0
+    if tails and (model_width % (tails + 1) or model_width // (tails + 1) % LANES):
+        tails = 0
+    if (tails + 1) * 2 * rows > LANES:
+        tails = 0
+    main = model_width - model_width // (tails + 1) if tails else model_width
 
     pieces, bits_of = mixer_weight[None], [0]
     batches = []
@@ -512,20 +625,21 @@
     joined_c = swap(joined, 1)
     joined_yc = swap(joined_y, 1)
     columns = lax.all_to_all(columns, "ep", 0, 0, tiled=True, axis_index_groups=z_groups)
+    project_options = dict(
+        scratch=[pltpu.VMEM((stations * seq_count, 4 * depth), F32)],
+        flops=2 * stations * seq_count * 2 * depth * wide,
+        moved=2 * depth * wide * 2,
+    )
+    (near,) = local_call(
+        functools.partial(project_kernel, (0, 1)),
+        [((stations * seq_count, wide), F32)],
+        **project_options,
+    )(columns, norm_gain[None], joined, joined_c)
     (partial,) = local_call(
-        project_kernel,
+        functools.partial(project_kernel, (2, 3)),
         [((stations, seq_count, wide), BF16)],
-        scratch=[
-            pltpu.VMEM((stations * seq_count, 4 * depth), F32),
-            pltpu.VMEM((4, depth, wide), BF16),
-            pltpu.VMEM((stations * seq_count, wide), F32),
-            pltpu.SemaphoreType.DMA((4,)),
-        ],
-        anywhere=(2, 3, 4, 5),
-        limit=60,
-        flops=2 * stations * seq_count * 4 * depth * wide,
-        moved=4 * depth * wide * 2,
-    )(columns, norm_gain[None], joined, joined_c, joined_y, joined_yc)
+        **project_options,
+    )(columns, norm_gain[None], joined_y, joined_yc, near)
     received = lax.all_to_all(partial, "ep", 0, 0, tiled=True, axis_index_groups=z_groups)
     for batch, bits in list(batches):
         batches.append((swap(batch, 2), [b ^ 2 for b in bits]))
@@ -534,11 +648,21 @@
     blocks = [batch for batch, _ in batches]
     places = tuple(tuple(bits) for _, bits in batches)
 
-    select, extra = local_call(
-        functools.partial(routing_kernel, group_width, rows),
-        [((seq_count, LANES), F32), ((seq_count, LANES), BF16)],
-    )(expert_index, route_weights)
-
+    select, side = local_call(
+        functools.partial(routing_kernel, group_width, limit, rows, tails),
+        [((seq_count, LANES), F32), ((seq_count, 2 * model_width + cell_width + 4 * LANES), F32)],
+        scratch=[pltpu.VMEM((LANES, LANES), F32)],
+        smem=(0, 1),
+    )(
+        ingate_bias, forget_bias, expert_index.T, route_weights.T, tokens, moe_gain[None],
+        normalizer, stabilizer.T,
+    )
+
+    others = []
+    for weight in (expert_gate, expert_up, expert_down):
+        others.append(swap(weight, 1))
+
+    heads = memory.shape[1]
     new_memory, new_normalizer, new_stabilizer, cell_out = local_call(
         cell_kernel,
         [
@@ -548,44 +672,47 @@
             ((seq_count, cell_width), BF16),
         ],
         scratch=[
-            pltpu.VMEM(memory.shape[1:2] + (LANES, LANES), F32),
-            pltpu.VMEM(memory.shape[1:2] + (LANES, LANES), F32),
+            pltpu.VMEM((heads, LANES, LANES), F32),
+            pltpu.VMEM((heads, LANES, LANES), BF16),
+            pltpu.VMEM((heads, 64, 2 * LANES), F32),
             pltpu.VMEM((seq_count, cell_width), F32),
             pltpu.VMEM((seq_count, cell_width), F32),
             pltpu.VMEM(memory.shape, F32),
             pltpu.SemaphoreType.DMA((seq_count,)),
         ],
         outs_hbm=(0,),
-        flops=6 * memory.size,
+        flops=4096 * memory.size,
         moved=8 * memory.size,
-        smem=(0, 1),
         limit=16,
-    )(ingate_bias, forget_bias, received, tokens, memory, normalizer, stabilizer)
-
+    )(received, memory, side)
     resid, outgoing = local_call(
         functools.partial(mix_kernel, places),
-        [((seq_count, model_width), F32), ((chips, rows, model_width + LANES), BF16)],
+        [((seq_count, model_width), F32), ((chips, rows, main + LANES), BF16)],
         scratch=[pltpu.VMEM((seq_count, model_width), F32)],
-        flops=2 * seq_count * cell_width * model_width,
+        flops=4096 * memory.size,
         moved=2 * cell_width * model_width,
         limit=12,
-    )(cell_out, tokens, moe_gain[None], select, extra, *blocks)
-
-    direct = lax.all_to_all(outgoing, "ep", 0, 0, tiled=True, axis_index_groups=chip_groups)
-    direct = direct.reshape(chips * rows, model_width + LANES)
-    across = swap(direct, 1)
-    kept, sent = local_call(
-        functools.partial(expert_kernel, group_width),
-        [((chips * rows, model_width), F32), ((chips * rows, model_width), BF16)],
+    )(cell_out, side, *blocks)
+
+    direct = lax.all_to_all(
+        outgoing, "ep", 0, 0, tiled=True, axis_index_groups=chip_groups
+    )
+    (summed,) = local_call(
+        functools.partial(expert_kernel, group_width, rows, limit, tails),
+        [((chips * rows, main), BF16)],
         flops=6 * 2 * chips * rows * model_width * expert_gate.shape[2],
         moved=6 * model_width * expert_gate.shape[2],
-        limit=24,
-    )(direct, across, expert_gate, expert_up, expert_down)
-    (summed,) = local_call(pair_kernel, [((chips * rows, model_width), BF16)])(kept, swap(sent, 1))
+        limit=12,
+    )(direct.reshape(chips * rows, main + LANES), expert_gate, expert_up, expert_down, *others)
     returned = lax.all_to_all(
-        summed.reshape(chips, rows, model_width), "ep", 0, 0, tiled=True, axis_index_groups=chip_groups
-    )
-    (layer_out,) = local_call(final_kernel, [((seq_count, model_width), BF16)])(returned, select, resid)
+        summed.reshape(chips, rows, main), "ep", 0, 0, tiled=True, axis_index_groups=chip_groups
+    )
+    (layer_out,) = local_call(
+        functools.partial(final_kernel, tails),
+        [((seq_count, model_width), BF16)],
+        scratch=[pltpu.VMEM((seq_count, model_width), F32), pltpu.SemaphoreType.DMA(())],
+        anywhere=(2,),
+    )(returned, select, resid)
     return (layer_out, new_memory, new_normalizer, new_stabilizer)
 
 

time: 104 us -> 94.8 us (0.912)
  waiting for transfers between devices: 40.2 us -> 27.7 us
  local copies, waits for them, and re-layouts: 4.1 us -> 6.42 us
  blocking collectives: 22 us -> 24.2 us
  starting transfers between devices: 18.8 us -> 17.6 us
    all_to_all x1, waiting for transfers between devices: 5.89 us -> 0.03 us  [on_device_fast(): lax.all_to_all(partial, 'ep', 0, 0, tiled=True, axis_index_groups=z_groups)]
    ppermute x13 -> x14, waiting for transfers between devices: 25.6 us -> 20.6 us  [swap(): return lax.ppermute(value, 'ep', [(i, i ^ bit) for i in range(size)])]
    unnamed x32 -> x41, local copies, waits for them, and re-layouts: 4.1 us -> 6.42 us
    all_to_all x1, blocking collectives: 11.4 us -> 13.7 us  [on_device_fast(): lax.all_to_all(outgoing, 'ep', 0, 0, tiled=True, axis_index_groups=chip_g...]
    all_to_all x1, waiting for transfers between devices: 8.77 us -> 7.06 us  [on_device_fast(): lax.all_to_all(summed.reshape(chips, rows, main), 'ep', 0, 0, tiled=True,...]
    ppermute x13 -> x14, starting transfers between devices: 11.9 us -> 10.8 us  [swap(): return lax.ppermute(value, 'ep', [(i, i ^ bit) for i in range(size)])]
  transfers between devices with their start and end apart: 15 -> 16, of which waited for: 6 -> 6; matrix products, arithmetic and copies ran while one was open for 2% -> 1% of each run, Pallas kernels for 10% -> 9%
where the time goes in v2:
time: 94.8 us; the launch traced here: 94.2 us
  waiting for transfers between devices  27.7 us (29%)
  blocking collectives  24.2 us (26%)
  starting transfers between devices  17.6 us (19%)
  Pallas kernels  17.3 us (18%)
  local copies, waits for them, and re-layouts  6.42 us (7%)
    ppermute x14, waiting for transfers between devices, swap(): return lax.ppermute(value, 'ep', [(i, i ^ bit) for i in range(size)])  20.6 us
    pallas_call x9, Pallas kernels, call(): pl.pallas_call(kernel, out_shape=[jax.ShapeDtypeStruct(*o) for o in outs]...  17.3 us
    all_to_all x1, blocking collectives, on_device_fast(): lax.all_to_all(outgoing, 'ep', 0, 0, tiled=True, axis_index_groups=chip_g...  13.7 us
    ppermute x14, starting transfers between devices, swap(): return lax.ppermute(value, 'ep', [(i, i ^ bit) for i in range(size)])  10.8 us
    all_to_all x1, blocking collectives, on_device_fast(): lax.all_to_all(columns, 'ep', 0, 0, tiled=True, axis_index_groups=z_groups)  10.5 us
    all_to_all x1, waiting for transfers between devices, on_device_fast(): lax.all_to_all(summed.reshape(chips, rows, main), 'ep', 0, 0, tiled=True,...  7.06 us
    unnamed x41, local copies, waits for them, and re-layouts  6.42 us
    all_to_all x1, starting transfers between devices, on_device_fast(): lax.all_to_all(partial, 'ep', 0, 0, tiled=True, axis_index_groups=z_groups)  3.45 us
  transfers between devices with their start and end apart: 16, of which 6 were waited for; matrix products, arithmetic and copies ran while one was open for 1% of the time, Pallas kernels for 9%

profile of v2, /device:TPU:0, one launch (start us, length us, event | category | flops | bytes accessed | tf_op | source)
XLA Modules:
  0.0 94.2 jit_solution(14555724178120003686)
XLA Ops:
  0.6 2.0 %shard_map.219 = (bf16[128,2176]{1,0:T(8,128)(2,1)}, bf16[4,12,512]{2,1,0:T(8,128)(2,1)}) custom-call(bf16[12,2048]{1,0:T(8,128)(2,1)} %tokens.3, bf16[128,512]{1,0:T(8,128)(2,1)} %query.1, bf16[128,512]{1,0:T(8,128)(2,1)} %key.1, bf16[128,512]{1,0:T(8,128)(2,1)} %value.1, bf16[128,512]{1,0:T(8,128)(2,1)} %outgate.1, bf16[4,128]{1,0:T(4,128)(2,1)} %bitcast.19, ...), custom_call_target="tpu_custom_call" | custom-call | flops 1 | bytes 1114112 | tf_op jit(solution)/shard_map/pallas_call | solution.py:187
  2.7 3.1 %collective-permute-start = (bf16[128,2176]{1,0:T(8,128)(2,1)}, bf16[128,2176]{1,0:T(8,128)(2,1)S(1)}, u32[]{:S(2)}, u32[]{:S(2)}) collective-permute-start(bf16[128,2176]{1,0:T(8,128)(2,1)} %get-tuple-element.15.first), channel_id=1, source_target_pairs={{0,2},{1,3},{2,0},{3,1},{4,6},{5,7},{6,4},{7,5},{8,10},{9,11},{10,... | collective-permute-start | bytes 1671176 | tf_op jit(solution)/shard_map/ppermute | solution.py:169
  5.7 1.6 %collective-permute-start.3 = (bf16[1,512,128]{2,1,0:T(8,128)(2,1)}, bf16[1,512,128]{2,1,0:T(8,128)(2,1)S(1)}, u32[]{:S(2)}, u32[]{:S(2)}) collective-permute-start(bf16[1,512,128]{2,1,0:T(8,128)(2,1)} %bitcast.17), channel_id=1, source_target_pairs={{0,4},{1,5},{2,6},{3,7},{4,0},{5,1},{6,2},{7,3},{8,12},{9,13},{10,... | collective-permute-start | bytes 393224 | tf_op jit(solution)/shard_map/ppermute | solution.py:169
  7.3 3.6 %collective-permute-done.3.second = bf16[1,512,128]{2,1,0:T(8,128)(2,1)S(1)} collective-permute-done((bf16[1,512,128]{2,1,0:T(8,128)(2,1)}, bf16[1,512,128]{2,1,0:T(8,128)(2,1)S(1)}, u32[]{:S(2)}, u32[]{:S(2)}) %collective-permute-start.3) | collective-permute-done | bytes 131104 | tf_op jit(solution)/shard_map/ppermute | solution.py:169
  11.6 1.7 %shard_map.224.refs_0_ = bf16[2,512,128]{2,1,0:T(8,128)(2,1)} custom-call(bf16[1,512,128]{2,1,0:T(8,128)(2,1)} %bitcast.18, bf16[1,512,128]{2,1,0:T(8,128)(2,1)} %copy-done.19), custom_call_target="tpu_custom_call" | custom-call | flops 1 | bytes 524288 | tf_op jit(solution)/shard_map/pallas_call | solution.py:187
  13.3 2.7 %collective-permute-start.4 = (bf16[2,512,128]{2,1,0:T(8,128)(2,1)}, bf16[2,512,128]{2,1,0:T(8,128)(2,1)S(1)}, u32[]{:S(2)}, u32[]{:S(2)}) collective-permute-start(bf16[2,512,128]{2,1,0:T(8,128)(2,1)} %shard_map.224.refs_0_), channel_id=1, source_target_pairs={{0,8},{1,9},{2,10},{3,11},{4,12},{5,13},{6,14},{7,15},{8,0},{9,1},... | collective-permute-start | bytes 786440 | tf_op jit(solution)/shard_map/ppermute | solution.py:169
  16.5 10.5 %collective-permute-done.4.refs_1_ = bf16[2,512,128]{2,1,0:T(8,128)(2,1)S(1)} collective-permute-done((bf16[2,512,128]{2,1,0:T(8,128)(2,1)}, bf16[2,512,128]{2,1,0:T(8,128)(2,1)S(1)}, u32[]{:S(2)}, u32[]{:S(2)}) %collective-permute-start.4) | collective-permute-done | bytes 262176 | tf_op jit(solution)/shard_map/ppermute | solution.py:169
  27.6 1.7 %collective-permute-done.2.second = bf16[128,2176]{1,0:T(8,128)(2,1)S(1)} collective-permute-done((bf16[128,2176]{1,0:T(8,128)(2,1)}, bf16[128,2176]{1,0:T(8,128)(2,1)S(1)}, u32[]{:S(2)}, u32[]{:S(2)}) %collective-permute-start.2) | collective-permute-done | bytes 557088 | tf_op jit(solution)/shard_map/ppermute | solution.py:169
  30.2 10.5 %all_to_all.20.columns = bf16[4,12,512]{2,1,0:T(8,128)(2,1)S(1)} all-to-all(bf16[4,12,512]{2,1,0:T(8,128)(2,1)} %get-tuple-element.14), channel_id=1, replica_groups={{0,4,8,12},{1,5,9,13},{2,6,10,14},{3,7,11,15},{16,20,24,28},{17,21,25,2..., dimensions={0} | all-to-all | bytes 98304 | tf_op jit(solution)/shard_map/all_to_all | solution.py:627
  40.7 1.1 %copy-done.3 = bf16[128,2176]{1,0:T(8,128)(2,1)S(1)} copy-done((bf16[128,2176]{1,0:T(8,128)(2,1)S(1)}, bf16[128,2176]{1,0:T(8,128)(2,1)}, u32[]{:S(2)}) %copy-start.3) | copy-done | bytes 557080
  42.7 1.0 %shard_map.221 = bf16[4,12,2176]{2,1,0:T(8,128)(2,1)} custom-call(bf16[4,12,512]{2,1,0:T(8,128)(2,1)S(1)} %all_to_all.20.columns, f32[1,2048]{1,0:T(1,128)S(1)} %bitcast.12, bf16[128,2176]{1,0:T(8,128)(2,1)S(1)} %collective-permute-done.first, bf16[128,2176]{1,0:T(8,128)(2,1)S(1)} %collective-permute-done.1.second, f32[48,2176]{1,0:T(8,128)S(1)} %shard_map.220.refs_0_), custom_call_target="tpu_custom_call" | custom-call | flops 53477376 | bytes 1114112 | tf_op jit(solution)/shard_map/pallas_call | solution.py:187
  43.8 3.5 %all-to-all-start.1 = ((bf16[4,12,2176]{2,1,0:T(8,128)(2,1)}), bf16[4,12,2176]{2,1,0:T(8,128)(2,1)S(1)}, u32[]{:S(2)}, u32[]{:S(2)}) async-start(bf16[4,12,2176]{2,1,0:T(8,128)(2,1)} %shard_map.221), calls=%async_computation.1 | async-start | bytes 557056 | tf_op jit(solution)/shard_map/all_to_all | solution.py:643
  47.2 1.2 %collective-permute-start.6 = (bf16[2,512,128]{2,1,0:T(8,128)(2,1)S(1)}, bf16[2,512,128]{2,1,0:T(8,128)(2,1)}, u32[]{:S(2)}, u32[]{:S(2)}) collective-permute-start(bf16[2,512,128]{2,1,0:T(8,128)(2,1)S(1)} %collective-permute-done.4.refs_1_), channel_id=1, source_target_pairs={{0,2},{1,3},{2,0},{3,1},{4,6},{5,7},{6,4},{7,5},{8,10},{9,11},{10,... | collective-permute-start | bytes 786440 | tf_op jit(solution)/shard_map/ppermute | solution.py:169
  48.4 0.7 copy-done.15
  49.2 0.8 shard_map.222
  50.0 4.7 %collective-permute-done.6.refs_3_ = bf16[2,512,128]{2,1,0:T(8,128)(2,1)} collective-permute-done((bf16[2,512,128]{2,1,0:T(8,128)(2,1)S(1)}, bf16[2,512,128]{2,1,0:T(8,128)(2,1)}, u32[]{:S(2)}, u32[]{:S(2)}) %collective-permute-start.6) | collective-permute-done | bytes 262176 | tf_op jit(solution)/shard_map/ppermute | solution.py:169
  55.9 1.9 %copy-done.14 = f32[12,4,128,128]{3,2,1,0:T(8,128)S(1)} copy-done((f32[12,4,128,128]{3,2,1,0:T(8,128)S(1)}, f32[12,4,128,128]{3,2,1,0:T(8,128)}, u32[]{:S(2)}) %copy-start.14) | copy-done | bytes 3145752
  57.8 3.0 %shard_map.223 = (f32[12,4,128,128]{3,2,1,0:T(8,128)}, f32[12,4,128]{2,1,0:T(4,128)}, f32[12,4]{1,0:T(8,128)S(1)}, bf16[12,512]{1,0:T(8,128)(2,1)S(1)}) custom-call(bf16[4,12,2176]{2,1,0:T(8,128)(2,1)S(1)} %all-to-all-done.1.received, f32[12,4,128,128]{3,2,1,0:T(8,128)S(1)} %copy-done.14, f32[12,5120]{1,0:T(8,128)S(1)} %get-tuple-element.16.side), custom_call_target="tpu_custom_call" | custom-call | flops 3221225472 | bytes 6291456 | tf_op jit(solution)/shard_map/pallas_call | solution.py:187
  60.9 1.9 %shard_map.225 = (f32[12,2048]{1,0:T(8,128)S(1)}, bf16[8,8,1664]{2,1,0:T(8,128)(2,1)S(1)}) custom-call(bf16[12,512]{1,0:T(8,128)(2,1)S(1)} %get-tuple-element.17.cell_out, f32[12,5120]{1,0:T(8,128)S(1)} %get-tuple-element.16.side, bf16[2,512,128]{2,1,0:T(8,128)(2,1)S(1)} %copy-done.5, bf16[2,512,128]{2,1,0:T(8,128)(2,1)S(1)} %collective-permute-done.4.refs_1_, ...), custom_call_target="tpu_custom_call" | custom-call | flops 3221225472 | bytes 2097152 | tf_op jit(solution)/shard_map/pallas_call | solution.py:187
  62.8 13.7 %all_to_all.21 = bf16[8,8,1664]{2,1,0:T(8,128)(2,1)S(1)} all-to-all(bf16[8,8,1664]{2,1,0:T(8,128)(2,1)S(1)} %get-tuple-element.18), channel_id=1, replica_groups={{0,2,4,6,8,10,12,14},{1,3,5,7,9,11,13,15},{16,18,20,22,24,26,28,30},{17..., dimensions={0} | all-to-all | bytes 425984 | tf_op jit(solution)/shard_map/all_to_all | solution.py:697
  76.5 5.5 %shard_map.226 = bf16[64,1536]{1,0:T(8,128)(2,1)} custom-call(bf16[64,1664]{1,0:T(8,128)(2,1)S(1)} %bitcast.10, bf16[1,2048,512]{2,1,0:T(8,128)(2,1)S(1)} %copy-done, bf16[1,2048,512]{2,1,0:T(8,128)(2,1)S(1)} %copy-done.1, bf16[1,512,2048]{2,1,0:T(8,128)(2,1)S(1)} %copy-done.2, bf16[1,2048,512]{2,1,0:T(8,128)(2,1)S(1)} %collective-permute-done.11.gate1, ...), custom_call_target="tpu_custom_call" | custom-call | flops 805306368 | bytes 6291456 | tf_op jit(solution)/shard_map/pallas_call | solution.py:187
  82.0 3.4 %all-to-all-start.3 = ((bf16[8,8,1536]{2,1,0:T(8,128)(2,1)}), bf16[8,8,1536]{2,1,0:T(8,128)(2,1)S(1)}, u32[]{:S(2)}, u32[]{:S(2)}) async-start(bf16[8,8,1536]{2,1,0:T(8,128)(2,1)} %bitcast.9), calls=%async_computation.3 | async-start | bytes 393216 | tf_op jit(solution)/shard_map/all_to_all | solution.py:707
  86.1 7.1 %all-to-all-done.3.returned = bf16[8,8,1536]{2,1,0:T(8,128)(2,1)S(1)} async-done(((bf16[8,8,1536]{2,1,0:T(8,128)(2,1)}), bf16[8,8,1536]{2,1,0:T(8,128)(2,1)S(1)}, u32[]{:S(2)}, u32[]{:S(2)}) %all-to-all-start.3) | async-done | bytes 196640 | tf_op jit(solution)/shard_map/all_to_all | solution.py:707
  93.1 1.0 %shard_map.227 = bf16[12,2048]{1,0:T(8,128)(2,1)} custom-call(bf16[8,8,1536]{2,1,0:T(8,128)(2,1)S(1)} %all-to-all-done.3.returned, f32[12,128]{1,0:T(8,128)S(1)} %get-tuple-element.19.select, f32[12,2048]{1,0:T(8,128)S(1)} %get-tuple-element.20.resid_far), custom_call_target="tpu_custom_call" | custom-call | flops 1 | bytes 1 | tf_op jit(solution)/shard_map/pallas_call | solution.py:187
  (60 shorter events, 5.6 us)
Async XLA Ops:
  2.7 24.4 %collective-permute-start = (bf16[128,2176]{1,0:T(8,128)(2,1)}, bf16[128,2176]{1,0:T(8,128)(2,1)S(1)}, u32[]{:S(2)}, u32[]{:S(2)}) collective-permute-start(bf16[128,2176]{1,0:T(8,128)(2,1)} %get-tuple-element.15.first), channel_id=1, source_target_pairs={{0,2},{1,3},{2,0},{3,1},{4,6},{5,7},{6,4},{7,5},{8,10},{9,11},{10,... | collective-permute-start | bytes 1671176 | tf_op jit(solution)/shard_map/ppermute | solution.py:169
  5.7 5.2 %collective-permute-start.3 = (bf16[1,512,128]{2,1,0:T(8,128)(2,1)}, bf16[1,512,128]{2,1,0:T(8,128)(2,1)S(1)}, u32[]{:S(2)}, u32[]{:S(2)}) collective-permute-start(bf16[1,512,128]{2,1,0:T(8,128)(2,1)} %bitcast.17), channel_id=1, source_target_pairs={{0,4},{1,5},{2,6},{3,7},{4,0},{5,1},{6,2},{7,3},{8,12},{9,13},{10,... | collective-permute-start | bytes 393224 | tf_op jit(solution)/shard_map/ppermute | solution.py:169
  13.3 35.9 %copy-start.4 = (bf16[12,2048]{1,0:T(8,128)(2,1)S(1)}, bf16[12,2048]{1,0:T(8,128)(2,1)}, u32[]{:S(2)}) copy-start(bf16[12,2048]{1,0:T(8,128)(2,1)} %tokens.3) | copy-start | bytes 147460
  13.3 35.8 %copy-start.7 = (f32[12,4,128]{2,1,0:T(4,128)S(1)}, f32[12,4,128]{2,1,0:T(4,128)}, u32[]{:S(2)}) copy-start(f32[12,4,128]{2,1,0:T(4,128)} %normalizer.1) | copy-start | bytes 73732
  13.3 35.8 %copy-start.8 = (f32[2048]{0:T(1024)S(1)}, f32[2048]{0:T(1024)}, u32[]{:S(2)}) copy-start(f32[2048]{0:T(1024)} %param.34) | copy-start | bytes 24580
  13.3 35.8 %copy-start.9 = (s32[12,6]{0,1:T(8,128)S(1)}, s32[12,6]{0,1:T(8,128)}, u32[]{:S(2)}) copy-start(s32[12,6]{0,1:T(8,128)} %param.38) | copy-start | bytes 868
  13.3 35.8 %copy-start.10 = (f32[12,6]{0,1:T(8,128)S(1)}, f32[12,6]{0,1:T(8,128)}, u32[]{:S(2)}) copy-start(f32[12,6]{0,1:T(8,128)} %param.39) | copy-start | bytes 868
  13.3 35.8 %copy-start.11 = (f32[12,4]{0,1:T(4,128)S(1)}, f32[12,4]{0,1:T(4,128)}, u32[]{:S(2)}) copy-start(f32[12,4]{0,1:T(4,128)} %param.32) | copy-start | bytes 580
  13.3 35.8 %copy-start.12 = (f32[4]{0:T(128)S(1)}, f32[4]{0:T(128)}, u32[]{:S(2)}) copy-start(f32[4]{0:T(128)} %ingate_bias.1) | copy-start | bytes 52
  13.3 35.8 %copy-start.13 = (f32[4]{0:T(128)S(1)}, f32[4]{0:T(128)}, u32[]{:S(2)}) copy-start(f32[4]{0:T(128)} %forget_bias.1) | copy-start | bytes 52
  13.3 13.7 %collective-permute-start.4 = (bf16[2,512,128]{2,1,0:T(8,128)(2,1)}, bf16[2,512,128]{2,1,0:T(8,128)(2,1)S(1)}, u32[]{:S(2)}, u32[]{:S(2)}) collective-permute-start(bf16[2,512,128]{2,1,0:T(8,128)(2,1)} %shard_map.224.refs_0_), channel_id=1, source_target_pairs={{0,8},{1,9},{2,10},{3,11},{4,12},{5,13},{6,14},{7,15},{8,0},{9,1},... | collective-permute-start | bytes 786440 | tf_op jit(solution)/shard_map/ppermute | solution.py:169
  16.0 60.5 %collective-permute-start.11 = (bf16[1,2048,512]{2,1,0:T(8,128)(2,1)}, bf16[1,2048,512]{2,1,0:T(8,128)(2,1)S(1)}, u32[]{:S(2)}, u32[]{:S(2)}) collective-permute-start(bf16[1,2048,512]{2,1,0:T(8,128)(2,1)} %gate0.1), channel_id=1, source_target_pairs={{0,1},{1,0},{2,3},{3,2},{4,5},{5,4},{6,7},{7,6},{8,9},{9,8},{10,11... | collective-permute-start | bytes 6291464 | tf_op jit(solution)/shard_map/ppermute | solution.py:169
  16.0 60.5 %collective-permute-start.12 = (bf16[1,2048,512]{2,1,0:T(8,128)(2,1)}, bf16[1,2048,512]{2,1,0:T(8,128)(2,1)}, u32[]{:S(2)}, u32[]{:S(2)}) collective-permute-start(bf16[1,2048,512]{2,1,0:T(8,128)(2,1)} %up0.1), channel_id=1, source_target_pairs={{0,1},{1,0},{2,3},{3,2},{4,5},{5,4},{6,7},{7,6},{8,9},{9,8},{10,11... | collective-permute-start | bytes 6291464 | tf_op jit(solution)/shard_map/ppermute | solution.py:169
  16.5 60.0 %collective-permute-start.13 = (bf16[1,512,2048]{2,1,0:T(8,128)(2,1)}, bf16[1,512,2048]{2,1,0:T(8,128)(2,1)}, u32[]{:S(2)}, u32[]{:S(2)}) collective-permute-start(bf16[1,512,2048]{2,1,0:T(8,128)(2,1)} %down0.1), channel_id=1, source_target_pairs={{0,1},{1,0},{2,3},{3,2},{4,5},{5,4},{6,7},{7,6},{8,9},{9,8},{10,11... | collective-permute-start | bytes 6291464 | tf_op jit(solution)/shard_map/ppermute | solution.py:169
  27.1 2.2 %collective-permute-start.2 = (bf16[128,2176]{1,0:T(8,128)(2,1)}, bf16[128,2176]{1,0:T(8,128)(2,1)S(1)}, u32[]{:S(2)}, u32[]{:S(2)}) collective-permute-start(bf16[128,2176]{1,0:T(8,128)(2,1)} %get-tuple-element.15.first), channel_id=1, source_target_pairs={{0,1},{1,0},{2,3},{3,2},{4,5},{5,4},{6,7},{7,6},{8,9},{9,8},{10,11... | collective-permute-start | bytes 1671176 | tf_op jit(solution)/shard_map/ppermute | solution.py:169
  27.1 3.0 %collective-permute-start.1 = (bf16[128,2176]{1,0:T(8,128)(2,1)S(1)}, bf16[128,2176]{1,0:T(8,128)(2,1)S(1)}, u32[]{:S(2)}, u32[]{:S(2)}) collective-permute-start(bf16[128,2176]{1,0:T(8,128)(2,1)S(1)} %collective-permute-done.first), channel_id=1, source_target_pairs={{0,1},{1,0},{2,3},{3,2},{4,5},{5,4},{6,7},{7,6},{8,9},{9,8},{10,11... | collective-permute-start | bytes 1671176 | tf_op jit(solution)/shard_map/ppermute | solution.py:169
  29.2 18.0 %collective-permute-start.5 = (bf16[2,512,128]{2,1,0:T(8,128)(2,1)}, bf16[2,512,128]{2,1,0:T(8,128)(2,1)S(1)}, u32[]{:S(2)}, u32[]{:S(2)}) collective-permute-start(bf16[2,512,128]{2,1,0:T(8,128)(2,1)} %shard_map.224.refs_0_), channel_id=1, source_target_pairs={{0,2},{1,3},{2,0},{3,1},{4,6},{5,7},{6,4},{7,5},{8,10},{9,11},{10,... | collective-permute-start | bytes 786440 | tf_op jit(solution)/shard_map/ppermute | solution.py:169
  30.0 18.4 %collective-permute-start.7 = (bf16[2,512,128]{2,1,0:T(8,128)(2,1)}, bf16[2,512,128]{2,1,0:T(8,128)(2,1)S(1)}, u32[]{:S(2)}, u32[]{:S(2)}) collective-permute-start(bf16[2,512,128]{2,1,0:T(8,128)(2,1)} %shard_map.224.refs_0_), channel_id=1, source_target_pairs={{0,1},{1,0},{2,3},{3,2},{4,5},{5,4},{6,7},{7,6},{8,9},{9,8},{10,11... | collective-permute-start | bytes 786440 | tf_op jit(solution)/shard_map/ppermute | solution.py:169
  43.8 12.1 %all-to-all-start.1 = ((bf16[4,12,2176]{2,1,0:T(8,128)(2,1)}), bf16[4,12,2176]{2,1,0:T(8,128)(2,1)S(1)}, u32[]{:S(2)}, u32[]{:S(2)}) async-start(bf16[4,12,2176]{2,1,0:T(8,128)(2,1)} %shard_map.221), calls=%async_computation.1 | async-start | bytes 557056 | tf_op jit(solution)/shard_map/all_to_all | solution.py:643
  47.2 7.4 %collective-permute-start.6 = (bf16[2,512,128]{2,1,0:T(8,128)(2,1)S(1)}, bf16[2,512,128]{2,1,0:T(8,128)(2,1)}, u32[]{:S(2)}, u32[]{:S(2)}) collective-permute-start(bf16[2,512,128]{2,1,0:T(8,128)(2,1)S(1)} %collective-permute-done.4.refs_1_), channel_id=1, source_target_pairs={{0,2},{1,3},{2,0},{3,1},{4,6},{5,7},{6,4},{7,5},{8,10},{9,11},{10,... | collective-permute-start | bytes 786440 | tf_op jit(solution)/shard_map/ppermute | solution.py:169
  49.1 5.6 %collective-permute-start.8 = (bf16[2,512,128]{2,1,0:T(8,128)(2,1)S(1)}, bf16[2,512,128]{2,1,0:T(8,128)(2,1)S(1)}, u32[]{:S(2)}, u32[]{:S(2)}) collective-permute-start(bf16[2,512,128]{2,1,0:T(8,128)(2,1)S(1)} %collective-permute-done.4.refs_1_), channel_id=1, source_target_pairs={{0,1},{1,0},{2,3},{3,2},{4,5},{5,4},{6,7},{7,6},{8,9},{9,8},{10,11... | collective-permute-start | bytes 786440 | tf_op jit(solution)/shard_map/ppermute | solution.py:169
  54.7 6.2 %collective-permute-start.9 = (bf16[2,512,128]{2,1,0:T(8,128)(2,1)S(1)}, bf16[2,512,128]{2,1,0:T(8,128)(2,1)}, u32[]{:S(2)}, u32[]{:S(2)}) collective-permute-start(bf16[2,512,128]{2,1,0:T(8,128)(2,1)S(1)} %collective-permute-done.5.refs_2_), channel_id=1, source_target_pairs={{0,1},{1,0},{2,3},{3,2},{4,5},{5,4},{6,7},{7,6},{8,9},{9,8},{10,11... | collective-permute-start | bytes 786440 | tf_op jit(solution)/shard_map/ppermute | solution.py:169
  55.4 5.5 %collective-permute-start.10 = (bf16[2,512,128]{2,1,0:T(8,128)(2,1)}, bf16[2,512,128]{2,1,0:T(8,128)(2,1)}, u32[]{:S(2)}, u32[]{:S(2)}) collective-permute-start(bf16[2,512,128]{2,1,0:T(8,128)(2,1)} %collective-permute-done.6.refs_3_), channel_id=1, source_target_pairs={{0,1},{1,0},{2,3},{3,2},{4,5},{5,4},{6,7},{7,6},{8,9},{9,8},{10,11... | collective-permute-start | bytes 786440 | tf_op jit(solution)/shard_map/ppermute | solution.py:169
  82.0 11.1 %all-to-all-start.3 = ((bf16[8,8,1536]{2,1,0:T(8,128)(2,1)}), bf16[8,8,1536]{2,1,0:T(8,128)(2,1)S(1)}, u32[]{:S(2)}, u32[]{:S(2)}) async-start(bf16[8,8,1536]{2,1,0:T(8,128)(2,1)} %bitcast.9), calls=%async_computation.3 | async-start | bytes 393216 | tf_op jit(solution)/shard_map/all_to_all | solution.py:707
  (12 other events, 61.8 us)

commit v3 on v2

--- a/solution.py
+++ b/solution.py
@@ -256,19 +256,24 @@
 
 
 def project_kernel(bits_of, columns, gain, first, second, *refs):
-    before, out, scaled = refs if len(refs) == 3 else (None,) + refs
     stations, rows, part = columns.shape
+    full = rows - 4
     depth = first.shape[0]
+    width = first.shape[1]
+    before, out, scaled, ends = refs if len(refs) == 4 else (None,) + refs
     me = lax.axis_index("ep")
     station, place = me // 4, me % 4
     gain_here = gain[:, pl.ds(pl.multiple_of(station * part, LANES), part)]
     for z in range(stations):
-        scaled[z * rows : (z + 1) * rows, :] = columns[z].astype(F32) * gain_here
+        x = columns[z].astype(F32) * gain_here
+        scaled[z * full : (z + 1) * full, :] = x[:full]
+        low = stations * full + z * 8
+        scaled[low : low + 4, :] = x[full:]
+        scaled[low + 4 : low + 8, :] = x[full:]
     parts = []
     for bits in bits_of:
         start = pl.multiple_of((place ^ bits) * depth, LANES)
         parts.append(scaled[:, pl.ds(start, depth)].astype(BF16))
-    width = out.shape[-1]
     step = 4 * LANES
     for low in range(0, width, step):
         high = min(low + step, width)
@@ -279,37 +284,58 @@
             continue
         term = term + before[:, low:high]
         for z in range(stations):
-            out[z, :, low:high] = term[z * rows : (z + 1) * rows].astype(BF16)
+            for f in range(full // 8):
+                start = z * full + f * 8
+                out[z, :, f * width + low : f * width + high] = term[start : start + 8].astype(BF16)
+        ends[:, low:high] = term[stations * full :]
+    if before is None:
+        return
+    split = left_width(width)
+    base = full // 8 * width
+    upper = lax.broadcasted_iota(jnp.int32, (8, width - split), 0) < 4
+    for z in range(stations):
+        end = ends[z * 8 : (z + 1) * 8, :]
+        paired = jnp.where(upper, end[:, : width - split], end[:, split:])
+        out[z, :, base : base + width - split] = paired.astype(BF16)
+        out[z, :, base + width - split :] = end[:, width - split : split].astype(BF16)
+
+
+def left_width(width):
+    return -(-width // (2 * LANES)) * LANES
+
+
+def unpacked(total, rows, width):
+    full = rows - 4
+    split = left_width(width)
+    tiles = [total[:, f * width : (f + 1) * width] for f in range(full // 8)]
+    base = full // 8 * width
+    left = total[0:4, base : base + split]
+    right = total[4:8, base : base + width - split]
+    return jnp.concatenate(tiles + [jnp.concatenate((left, right), axis=1)], axis=0)
 
 
 def rounded(value):
     return value.astype(BF16).astype(F32)
 
 
-def cell_kernel(
-    received, memory, side, new_memory, new_normalizer, new_stabilizer, cell_out,
-    turned, flipped, spread, keeps, numer, fresh, sems,
+def gate_kernel(
+    rows, heads, received, side, new_normalizer, new_stabilizer,
+    flipped, spread, keeps, factor, turned, values,
 ):
-    stations, rows, _ = received.shape
-    heads = memory.shape[1]
-    dim = memory.shape[2]
-    width = heads * dim
-    low = side.shape[1] - 4 * LANES
-    model_width = (low - width) // 2
-    scale = side[:, low : low + 1]
-    known = side[:, low + 2 * LANES : low + 3 * LANES]
+    stations = received.shape[0]
+    width = keeps.shape[1]
+    dim = width // heads
+    scale = side[:, width : width + 1]
+    known = side[:, width + LANES : width + 2 * LANES]
     total = received[0].astype(F32)
     for z in range(1, stations):
         total = total + received[z].astype(F32)
-    total = total * scale
+    total = unpacked(total, rows, 4 * width + LANES) * scale
     gates = total[:, 4 * width :]
-    value = rounded(total[:, 2 * width : 3 * width])
+    turned[...] = jnp.zeros_like(turned)
+    values[...] = jnp.zeros_like(values)
     lane = lax.broadcasted_iota(jnp.int32, (rows, heads), 1)
     states = jnp.zeros((rows, heads), F32)
-    denoms = []
-    turned[...] = jnp.zeros_like(turned)
-    spread[...] = jnp.zeros_like(spread)
-    spread[:, 0:16, 0:dim] = jnp.ones((heads, 16, dim), F32)
     for h in range(heads):
         cut = slice(h * dim, (h + 1) * dim)
         query = rounded(total[:, h * dim : (h + 1) * dim])
@@ -323,10 +349,11 @@
         keep = jnp.broadcast_to(jnp.exp(carried - state), (rows, dim))
         keeps[:, cut] = keep
         write_key = jnp.exp(ingate_pre - state) * key
-        base = 2 * model_width + h * dim
-        normal = keep * side[:, base : base + dim] + write_key
+        normal = keep * side[:, cut] + write_key
         new_normalizer[:, h, :] = normal
-        denoms.append(jnp.sum(query * normal, axis=-1, keepdims=True))
+        denom = jnp.sum(query * normal, axis=-1, keepdims=True)
+        outgate = rounded(total[:, 3 * width + h * dim : 3 * width + (h + 1) * dim])
+        factor[:, cut] = 1.0 / (jnp.maximum(jnp.abs(denom), 1.0) * (1.0 + jnp.exp(-outgate)))
         high = rounded(write_key)
         middle = rounded(write_key - high)
         turned[h, 0:rows, :] = query
@@ -334,12 +361,22 @@
         turned[h, 32 : 32 + rows, :] = middle
         turned[h, 48 : 48 + rows, :] = rounded(write_key - high - middle)
         flipped[h] = turned[h].T.astype(BF16)
+        value = total[:, 2 * width + h * dim : 2 * width + (h + 1) * dim]
         for i in range(1, 4):
-            spread[h, 16 * i : 16 * i + rows, dim:] = value[:, cut]
+            values[16 * i : 16 * i + rows, :] = value
+        spread[h, :, dim:] = values[...].astype(BF16)
+        which = lax.broadcasted_iota(jnp.int32, (64, dim), 0)
+        spread[h, :, :dim] = jnp.where(which < 16, 1.0, 0.0).astype(BF16)
     new_stabilizer[...] = states
+
+
+def cell_kernel(
+    flipped, spread, keeps, factor, memory, new_memory, cell_out, numer, fresh, sems
+):
+    rows, heads, dim = memory.shape[:3]
     copies = []
     which = lax.broadcasted_iota(jnp.int32, (64, 2 * dim), 0) % 16
-    spreads = [spread[h].astype(BF16) for h in range(heads)]
+    spreads = [spread[h] for h in range(heads)]
     for t in range(rows):
         for h in range(heads):
             cut = slice(h * dim, (h + 1) * dim)
@@ -350,22 +387,15 @@
             numer[t : t + 1, cut] = jnp.sum(both[:, :dim] * block, axis=0, keepdims=True)
         copies.append(pltpu.make_async_copy(fresh.at[t], new_memory.at[t], sems.at[t]))
         copies[-1].start()
-    for h in range(heads):
-        cut = slice(h * dim, (h + 1) * dim)
-        outgate = rounded(total[:, 3 * width + h * dim : 3 * width + (h + 1) * dim])
-        hidden = numer[:, cut] / jnp.maximum(jnp.abs(denoms[h]), 1.0)
-        cell_out[:, cut] = (hidden / (1.0 + jnp.exp(-outgate))).astype(BF16)
+    cell_out[...] = (numer[...] * factor[...]).astype(BF16)
     for copy in copies:
         copy.wait()
 
 
-def mix_kernel(places, cell_out, side, *refs):
+def mix_kernel(places, cell_out, side, select, tokens, gain, *refs):
     blocks, (resid, outgoing, mixed) = refs[: len(places)], refs[len(places) :]
     cell = cell_out[...]
-    model_width = resid.shape[1]
-    low = side.shape[1] - 4 * LANES
-    select = side[:, low + LANES : low + 2 * LANES]
-    extra = side[:, low + 3 * LANES : low + 4 * LANES].astype(BF16)
+    extra = side[:, side.shape[1] - LANES :].astype(BF16)
     me = lax.axis_index("ep")
     piece = blocks[0].shape[2]
     for i, bits_of in enumerate(places):
@@ -373,10 +403,10 @@
             block = jnp.dot(cell, blocks[i][number], preferred_element_type=F32)
             start = pl.multiple_of((me ^ bits) * piece, LANES)
             mixed[:, pl.ds(start, piece)] = rounded(block)
-    level = side[:, 0:model_width] + mixed[...]
+    level = tokens[...].astype(F32) + mixed[...]
     resid[...] = level
     scale = lax.rsqrt(jnp.mean(level * level, axis=-1, keepdims=True) + EPS)
-    moe_in = (level * scale * side[:, model_width : 2 * model_width]).astype(BF16)
+    moe_in = (level * scale * gain[...]).astype(BF16)
     chips, rows_pad, packed = outgoing.shape
     main = packed - LANES
     tail = moe_in.shape[1] - main
@@ -405,17 +435,14 @@
 
 def routing_kernel(
     group_width, limit, rows_pad, tails,
-    ingate_bias, forget_bias, index, weights, tokens, gain, normalizer, stabilizer,
+    ingate_bias, forget_bias, index, weights, tokens, normalizer, stabilizer,
     select, side, small,
 ):
     chosen, rows = index.shape
     heads, dim = normalizer.shape[1:]
-    width = tokens.shape[1]
     stream = tokens[...].astype(F32)
     scale = lax.rsqrt(jnp.mean(stream * stream, axis=-1, keepdims=True) + EPS)
-    side[:, 0:width] = stream
-    side[:, width : 2 * width] = jnp.broadcast_to(gain[...], (rows, width))
-    low = 2 * width
+    low = 0
     for h in range(heads):
         side[:, low : low + dim] = normalizer[:, h, :]
         low += dim
@@ -448,8 +475,7 @@
             lane == (1.0 + within) * (2 * rows_pad) + base + limit + turn
         )
     select[...] = chosen_lanes.astype(F32)
-    side[:, low + LANES : low + 2 * LANES] = chosen_lanes.astype(F32)
-    side[:, low + 2 * LANES : low + 3 * LANES] = flat[0:rows, :]
+    side[:, low + LANES : low + 2 * LANES] = flat[0:rows, :]
     dense = jnp.zeros((rows, LANES), F32)
     for k in range(chosen):
         expert = experts[:, k : k + 1]
@@ -457,7 +483,7 @@
         hit = (lane == local) | (lane == local + group_width)
         dense = dense + jnp.where(hit, flat[0:rows, 64 + k : 65 + k], 0.0)
     high = rounded(dense)
-    side[:, low + 3 * LANES : low + 4 * LANES] = jnp.where(lane < group_width, high, dense - high)
+    side[:, low + 2 * LANES : low + 3 * LANES] = jnp.where(lane < group_width, high, dense - high)
 
 
 def sorted_rows(count, rows_pad, limit, tails, j, back):
@@ -625,19 +651,24 @@
     joined_c = swap(joined, 1)
     joined_yc = swap(joined_y, 1)
     columns = lax.all_to_all(columns, "ep", 0, 0, tiled=True, axis_index_groups=z_groups)
+    message = (seq_count - 4) // 8 * wide + left_width(wide)
+    project_rows = stations * (seq_count + 4)
     project_options = dict(
-        scratch=[pltpu.VMEM((stations * seq_count, 4 * depth), F32)],
+        scratch=[
+            pltpu.VMEM((project_rows, 4 * depth), F32),
+            pltpu.VMEM((stations * 8, wide), F32),
+        ],
         flops=2 * stations * seq_count * 2 * depth * wide,
         moved=2 * depth * wide * 2,
     )
     (near,) = local_call(
         functools.partial(project_kernel, (0, 1)),
-        [((stations * seq_count, wide), F32)],
+        [((project_rows, wide), F32)],
         **project_options,
     )(columns, norm_gain[None], joined, joined_c)
     (partial,) = local_call(
         functools.partial(project_kernel, (2, 3)),
-        [((stations, seq_count, wide), BF16)],
+        [((stations, 8, message), BF16)],
         **project_options,
     )(columns, norm_gain[None], joined_y, joined_yc, near)
     received = lax.all_to_all(partial, "ep", 0, 0, tiled=True, axis_index_groups=z_groups)
@@ -650,11 +681,14 @@
 
     select, side = local_call(
         functools.partial(routing_kernel, group_width, limit, rows, tails),
-        [((seq_count, LANES), F32), ((seq_count, 2 * model_width + cell_width + 4 * LANES), F32)],
+        [
+            ((seq_count, LANES), F32),
+            ((seq_count, cell_width + 3 * LANES), F32),
+        ],
         scratch=[pltpu.VMEM((LANES, LANES), F32)],
         smem=(0, 1),
     )(
-        ingate_bias, forget_bias, expert_index.T, route_weights.T, tokens, moe_gain[None],
+        ingate_bias, forget_bias, expert_index.T, route_weights.T, tokens,
         normalizer, stabilizer.T,
     )
 
@@ -663,19 +697,26 @@
         others.append(swap(weight, 1))
 
     heads = memory.shape[1]
-    new_memory, new_normalizer, new_stabilizer, cell_out = local_call(
-        cell_kernel,
+    new_normalizer, new_stabilizer, *turned = local_call(
+        functools.partial(gate_kernel, seq_count, heads),
         [
-            (memory.shape, F32),
             (normalizer.shape, F32),
             (stabilizer.shape, F32),
-            ((seq_count, cell_width), BF16),
+            ((heads, LANES, LANES), BF16),
+            ((heads, 64, 2 * LANES), BF16),
+            ((seq_count, cell_width), F32),
+            ((seq_count, cell_width), F32),
         ],
         scratch=[
             pltpu.VMEM((heads, LANES, LANES), F32),
-            pltpu.VMEM((heads, LANES, LANES), BF16),
-            pltpu.VMEM((heads, 64, 2 * LANES), F32),
-            pltpu.VMEM((seq_count, cell_width), F32),
+            pltpu.VMEM((64, LANES), F32),
+        ],
+        flops=4096 * memory.size,
+    )(received, side)
+    new_memory, cell_out = local_call(
+        cell_kernel,
+        [(memory.shape, F32), ((seq_count, cell_width), BF16)],
+        scratch=[
             pltpu.VMEM((seq_count, cell_width), F32),
             pltpu.VMEM(memory.shape, F32),
             pltpu.SemaphoreType.DMA((seq_count,)),
@@ -683,8 +724,8 @@
         outs_hbm=(0,),
         flops=4096 * memory.size,
         moved=8 * memory.size,
-        limit=16,
-    )(received, memory, side)
+        limit=12,
+    )(*turned, memory)
     resid, outgoing = local_call(
         functools.partial(mix_kernel, places),
         [((seq_count, model_width), F32), ((chips, rows, main + LANES), BF16)],
@@ -692,7 +733,7 @@
         flops=4096 * memory.size,
         moved=2 * cell_width * model_width,
         limit=12,
-    )(cell_out, side, *blocks)
+    )(cell_out, side, select, tokens, moe_gain[None], *blocks)
 
     direct = lax.all_to_all(
         outgoing, "ep", 0, 0, tiled=True, axis_index_groups=chip_groups
@@ -721,7 +762,8 @@
     aligned = ep_size % 8 == 0 and ep_size <= 16
 
     def run(*arrays):
-        fits = aligned and arrays[13].shape[1] // ep_size % 128 == 0 and arrays[15].shape[0] == ep_size
+        fits = aligned and arrays[0].shape[0] // mesh.size % 8 == 4
+        fits = fits and arrays[13].shape[1] // ep_size % 128 == 0 and arrays[15].shape[0] == ep_size
         fits = fits and arrays[2].shape[0] // ep_size % 128 == 0 and arrays[10].shape[2] == 128
 
         def body(*blocks):

time: 94.8 us -> 98.4 us (1.038)
  blocking collectives: 24.2 us -> 28 us
  starting transfers between devices: 17.6 us -> 20.3 us
  local copies, waits for them, and re-layouts: 6.42 us -> 4.01 us
    all_to_all x1, blocking collectives: 10.5 us -> 14.2 us  [on_device_fast(): lax.all_to_all(columns, 'ep', 0, 0, tiled=True, axis_index_groups=z_groups)]
    unnamed x41 -> x33, local copies, waits for them, and re-layouts: 6.42 us -> 4.01 us
    all_to_all x1, starting transfers between devices: 3.45 us -> 4.82 us  [on_device_fast(): lax.all_to_all(partial, 'ep', 0, 0, tiled=True, axis_index_groups=z_groups)]
    ppermute x14, starting transfers between devices: 10.8 us -> 12.1 us  [swap(): return lax.ppermute(value, 'ep', [(i, i ^ bit) for i in range(size)])]
    pallas_call x9 -> x10, Pallas kernels: 17.3 us -> 17.1 us  [call(): pl.pallas_call(kernel, out_shape=[jax.ShapeDtypeStruct(*o) for o in outs]...]
  transfers between devices with their start and end apart: 16 -> 16, of which waited for: 6 -> 4; matrix products, arithmetic and copies ran while one was open for 1% -> 1% of each run, Pallas kernels for 9% -> 9%
where the time goes in v3:
time: 98.4 us; the launch traced here: 97.8 us
  blocking collectives  28 us (28%)
  waiting for transfers between devices  27.4 us (28%)
  starting transfers between devices  20.3 us (21%)
  Pallas kernels  17.1 us (17%)
  local copies, waits for them, and re-layouts  4.01 us (4%)
    ppermute x14, waiting for transfers between devices, swap(): return lax.ppermute(value, 'ep', [(i, i ^ bit) for i in range(size)])  20.4 us
    pallas_call x10, Pallas kernels, call(): pl.pallas_call(kernel, out_shape=[jax.ShapeDtypeStruct(*o) for o in outs]...  17.1 us
    all_to_all x1, blocking collectives, on_device_fast(): lax.all_to_all(columns, 'ep', 0, 0, tiled=True, axis_index_groups=z_groups)  14.2 us
    all_to_all x1, blocking collectives, on_device_fast(): lax.all_to_all(outgoing, 'ep', 0, 0, tiled=True, axis_index_groups=chip_g...  13.8 us
    ppermute x14, starting transfers between devices, swap(): return lax.ppermute(value, 'ep', [(i, i ^ bit) for i in range(size)])  12.1 us
    all_to_all x1, waiting for transfers between devices, on_device_fast(): lax.all_to_all(summed.reshape(chips, rows, main), 'ep', 0, 0, tiled=True,...  7.06 us
    all_to_all x1, starting transfers between devices, on_device_fast(): lax.all_to_all(partial, 'ep', 0, 0, tiled=True, axis_index_groups=z_groups)  4.82 us
    unnamed x33, local copies, waits for them, and re-layouts  4.01 us
  transfers between devices with their start and end apart: 16, of which 4 were waited for; matrix products, arithmetic and copies ran while one was open for 1% of the time, Pallas kernels for 9%

profile of v3, /device:TPU:0, one launch (start us, length us, event | category | flops | bytes accessed | tf_op | source)
XLA Modules:
  0.0 97.8 jit_solution(5520994542029021171)
XLA Ops:
  0.6 2.0 %shard_map.219 = (bf16[128,2176]{1,0:T(8,128)(2,1)}, bf16[4,12,512]{2,1,0:T(8,128)(2,1)}) custom-call(bf16[12,2048]{1,0:T(8,128)(2,1)} %tokens.5, bf16[128,512]{1,0:T(8,128)(2,1)} %query.1, bf16[128,512]{1,0:T(8,128)(2,1)} %key.1, bf16[128,512]{1,0:T(8,128)(2,1)} %value.1, bf16[128,512]{1,0:T(8,128)(2,1)} %outgate.1, bf16[4,128]{1,0:T(4,128)(2,1)} %bitcast.19, ...), custom_call_target="tpu_custom_call" | custom-call | flops 1 | bytes 1114112 | tf_op jit(solution)/shard_map/pallas_call | solution.py:187
  2.7 3.1 %collective-permute-start = (bf16[128,2176]{1,0:T(8,128)(2,1)}, bf16[128,2176]{1,0:T(8,128)(2,1)S(1)}, u32[]{:S(2)}, u32[]{:S(2)}) collective-permute-start(bf16[128,2176]{1,0:T(8,128)(2,1)} %get-tuple-element.19.first), channel_id=1, source_target_pairs={{0,2},{1,3},{2,0},{3,1},{4,6},{5,7},{6,4},{7,5},{8,10},{9,11},{10,... | collective-permute-start | bytes 1671176 | tf_op jit(solution)/shard_map/ppermute | solution.py:169
  5.7 1.6 %collective-permute-start.3 = (bf16[1,512,128]{2,1,0:T(8,128)(2,1)}, bf16[1,512,128]{2,1,0:T(8,128)(2,1)S(1)}, u32[]{:S(2)}, u32[]{:S(2)}) collective-permute-start(bf16[1,512,128]{2,1,0:T(8,128)(2,1)} %bitcast.17), channel_id=1, source_target_pairs={{0,4},{1,5},{2,6},{3,7},{4,0},{5,1},{6,2},{7,3},{8,12},{9,13},{10,... | collective-permute-start | bytes 393224 | tf_op jit(solution)/shard_map/ppermute | solution.py:169
  7.3 11.3 %collective-permute-done.first = bf16[128,2176]{1,0:T(8,128)(2,1)S(1)} collective-permute-done((bf16[128,2176]{1,0:T(8,128)(2,1)}, bf16[128,2176]{1,0:T(8,128)(2,1)S(1)}, u32[]{:S(2)}, u32[]{:S(2)}) %collective-permute-start) | collective-permute-done | bytes 557088 | tf_op jit(solution)/shard_map/ppermute | solution.py:169
  19.7 1.7 %shard_map.225.refs_0_ = bf16[2,512,128]{2,1,0:T(8,128)(2,1)} custom-call(bf16[1,512,128]{2,1,0:T(8,128)(2,1)} %bitcast.18, bf16[1,512,128]{2,1,0:T(8,128)(2,1)} %copy-done.15), custom_call_target="tpu_custom_call" | custom-call | flops 1 | bytes 524288 | tf_op jit(solution)/shard_map/pallas_call | solution.py:187
  21.5 2.9 %collective-permute-start.4 = (bf16[2,512,128]{2,1,0:T(8,128)(2,1)}, bf16[2,512,128]{2,1,0:T(8,128)(2,1)}, u32[]{:S(2)}, u32[]{:S(2)}) collective-permute-start(bf16[2,512,128]{2,1,0:T(8,128)(2,1)} %shard_map.225.refs_0_), channel_id=1, source_target_pairs={{0,8},{1,9},{2,10},{3,11},{4,12},{5,13},{6,14},{7,15},{8,0},{9,1},... | collective-permute-start | bytes 786440 | tf_op jit(solution)/shard_map/ppermute | solution.py:169
  24.3 14.2 %all_to_all.20.columns = bf16[4,12,512]{2,1,0:T(8,128)(2,1)S(1)} all-to-all(bf16[4,12,512]{2,1,0:T(8,128)(2,1)} %get-tuple-element.18), channel_id=1, replica_groups={{0,4,8,12},{1,5,9,13},{2,6,10,14},{3,7,11,15},{16,20,24,28},{17,21,25,2..., dimensions={0} | all-to-all | bytes 98304 | tf_op jit(solution)/shard_map/all_to_all | solution.py:653
  38.6 1.1 %copy-done.3 = bf16[128,2176]{1,0:T(8,128)(2,1)S(1)} copy-done((bf16[128,2176]{1,0:T(8,128)(2,1)S(1)}, bf16[128,2176]{1,0:T(8,128)(2,1)}, u32[]{:S(2)}) %copy-start.3) | copy-done | bytes 557080
  40.7 1.0 %shard_map.221 = bf16[4,8,3328]{2,1,0:T(8,128)(2,1)} custom-call(bf16[4,12,512]{2,1,0:T(8,128)(2,1)S(1)} %all_to_all.20.columns, f32[1,2048]{1,0:T(1,128)S(1)} %bitcast.12, bf16[128,2176]{1,0:T(8,128)(2,1)S(1)} %collective-permute-done.first, bf16[128,2176]{1,0:T(8,128)(2,1)S(1)} %collective-permute-done.1.second, f32[64,2176]{1,0:T(8,128)S(1)} %shard_map.220.refs_0_), custom_call_target="tpu_custom_call" | custom-call | flops 53477376 | bytes 1114112 | tf_op jit(solution)/shard_map/pallas_call | solution.py:187
  41.7 4.8 %all-to-all-start.1 = ((bf16[4,8,3328]{2,1,0:T(8,128)(2,1)}), bf16[4,8,3328]{2,1,0:T(8,128)(2,1)S(1)}, u32[]{:S(2)}, u32[]{:S(2)}) async-start(bf16[4,8,3328]{2,1,0:T(8,128)(2,1)} %shard_map.221), calls=%async_computation.1 | async-start | bytes 425984 | tf_op jit(solution)/shard_map/all_to_all | solution.py:674
  46.5 1.5 %collective-permute-start.5 = (bf16[2,512,128]{2,1,0:T(8,128)(2,1)S(1)}, bf16[2,512,128]{2,1,0:T(8,128)(2,1)S(1)}, u32[]{:S(2)}, u32[]{:S(2)}) collective-permute-start(bf16[2,512,128]{2,1,0:T(8,128)(2,1)S(1)} %copy-done.5), channel_id=1, source_target_pairs={{0,2},{1,3},{2,0},{3,1},{4,6},{5,7},{6,4},{7,5},{8,10},{9,11},{10,... | collective-permute-start | bytes 786440 | tf_op jit(solution)/shard_map/ppermute | solution.py:169
  48.1 0.7 copy-done.7
  49.5 0.8 shard_map.222
  50.3 4.2 %collective-permute-done.5.refs_2_ = bf16[2,512,128]{2,1,0:T(8,128)(2,1)S(1)} collective-permute-done((bf16[2,512,128]{2,1,0:T(8,128)(2,1)S(1)}, bf16[2,512,128]{2,1,0:T(8,128)(2,1)S(1)}, u32[]{:S(2)}, u32[]{:S(2)}) %collective-permute-start.5) | collective-permute-done | bytes 262176 | tf_op jit(solution)/shard_map/ppermute | solution.py:169
  54.5 1.5 %collective-permute-start.6 = (bf16[2,512,128]{2,1,0:T(8,128)(2,1)}, bf16[2,512,128]{2,1,0:T(8,128)(2,1)S(1)}, u32[]{:S(2)}, u32[]{:S(2)}) collective-permute-start(bf16[2,512,128]{2,1,0:T(8,128)(2,1)} %collective-permute-done.4.refs_1_), channel_id=1, source_target_pairs={{0,2},{1,3},{2,0},{3,1},{4,6},{5,7},{6,4},{7,5},{8,10},{9,11},{10,... | collective-permute-start | bytes 786440 | tf_op jit(solution)/shard_map/ppermute | solution.py:169
  56.1 0.9 shard_map.223
  57.0 4.9 %collective-permute-done.6.refs_3_ = bf16[2,512,128]{2,1,0:T(8,128)(2,1)S(1)} collective-permute-done((bf16[2,512,128]{2,1,0:T(8,128)(2,1)}, bf16[2,512,128]{2,1,0:T(8,128)(2,1)S(1)}, u32[]{:S(2)}, u32[]{:S(2)}) %collective-permute-start.6) | collective-permute-done | bytes 262176 | tf_op jit(solution)/shard_map/ppermute | solution.py:169
  62.4 2.0 %shard_map.224 = (f32[12,4,128,128]{3,2,1,0:T(8,128)}, bf16[12,512]{1,0:T(8,128)(2,1)S(1)}) custom-call(bf16[4,128,128]{2,1,0:T(8,128)(2,1)S(1)} %get-tuple-element.21.flipped, bf16[4,64,256]{2,1,0:T(8,128)(2,1)S(1)} %get-tuple-element.22.spread, f32[12,512]{1,0:T(8,128)S(1)} %get-tuple-element.23.keeps, f32[12,512]{1,0:T(8,128)S(1)} %get-tuple-element.24.factor, ...), custom_call_target="tpu_custom_call" | custom-call | flops 3221225472 | bytes 6291456 | tf_op jit(solution)/shard_map/pallas_call | solution.py:187
  64.4 1.8 %shard_map.226 = (f32[12,2048]{1,0:T(8,128)S(1)}, bf16[8,8,1664]{2,1,0:T(8,128)(2,1)S(1)}) custom-call(bf16[12,512]{1,0:T(8,128)(2,1)S(1)} %get-tuple-element.25.cell_out, f32[12,896]{1,0:T(8,128)S(1)} %get-tuple-element.20.side, f32[12,128]{1,0:T(8,128)S(1)} %get-tuple-element.26.select, bf16[12,2048]{1,0:T(8,128)(2,1)S(1)} %copy-done.4, ...), custom_call_target="tpu_custom_call" | custom-call | flops 3221225472 | bytes 2097152 | tf_op jit(solution)/shard_map/pallas_call | solution.py:187
  66.3 13.8 %all_to_all.21 = bf16[8,8,1664]{2,1,0:T(8,128)(2,1)S(1)} all-to-all(bf16[8,8,1664]{2,1,0:T(8,128)(2,1)S(1)} %get-tuple-element.27), channel_id=1, replica_groups={{0,2,4,6,8,10,12,14},{1,3,5,7,9,11,13,15},{16,18,20,22,24,26,28,30},{17..., dimensions={0} | all-to-all | bytes 425984 | tf_op jit(solution)/shard_map/all_to_all | solution.py:738
  80.1 5.5 %shard_map.227 = bf16[64,1536]{1,0:T(8,128)(2,1)} custom-call(bf16[64,1664]{1,0:T(8,128)(2,1)S(1)} %bitcast.10, bf16[1,2048,512]{2,1,0:T(8,128)(2,1)S(1)} %copy-done, bf16[1,2048,512]{2,1,0:T(8,128)(2,1)S(1)} %copy-done.1, bf16[1,512,2048]{2,1,0:T(8,128)(2,1)S(1)} %copy-done.2, bf16[1,2048,512]{2,1,0:T(8,128)(2,1)S(1)} %collective-permute-done.11.gate1, ...), custom_call_target="tpu_custom_call" | custom-call | flops 805306368 | bytes 6291456 | tf_op jit(solution)/shard_map/pallas_call | solution.py:187
  85.6 3.4 %all-to-all-start.3 = ((bf16[8,8,1536]{2,1,0:T(8,128)(2,1)}), bf16[8,8,1536]{2,1,0:T(8,128)(2,1)S(1)}, u32[]{:S(2)}, u32[]{:S(2)}) async-start(bf16[8,8,1536]{2,1,0:T(8,128)(2,1)} %bitcast.9), calls=%async_computation.3 | async-start | bytes 393216 | tf_op jit(solution)/shard_map/all_to_all | solution.py:748
  89.7 7.1 %all-to-all-done.3.returned = bf16[8,8,1536]{2,1,0:T(8,128)(2,1)S(1)} async-done(((bf16[8,8,1536]{2,1,0:T(8,128)(2,1)}), bf16[8,8,1536]{2,1,0:T(8,128)(2,1)S(1)}, u32[]{:S(2)}, u32[]{:S(2)}) %all-to-all-start.3) | async-done | bytes 196640 | tf_op jit(solution)/shard_map/all_to_all | solution.py:748
  96.7 1.0 %shard_map.228 = bf16[12,2048]{1,0:T(8,128)(2,1)} custom-call(bf16[8,8,1536]{2,1,0:T(8,128)(2,1)S(1)} %all-to-all-done.3.returned, f32[12,128]{1,0:T(8,128)S(1)} %get-tuple-element.26.select, f32[12,2048]{1,0:T(8,128)S(1)} %get-tuple-element.28.resid_far), custom_call_target="tpu_custom_call" | custom-call | flops 1 | bytes 1 | tf_op jit(solution)/shard_map/pallas_call | solution.py:187
  (53 shorter events, 4.1 us)
Async XLA Ops:
  2.7 15.9 %collective-permute-start = (bf16[128,2176]{1,0:T(8,128)(2,1)}, bf16[128,2176]{1,0:T(8,128)(2,1)S(1)}, u32[]{:S(2)}, u32[]{:S(2)}) collective-permute-start(bf16[128,2176]{1,0:T(8,128)(2,1)} %get-tuple-element.19.first), channel_id=1, source_target_pairs={{0,2},{1,3},{2,0},{3,1},{4,6},{5,7},{6,4},{7,5},{8,10},{9,11},{10,... | collective-permute-start | bytes 1671176 | tf_op jit(solution)/shard_map/ppermute | solution.py:169
  5.7 15.7 %collective-permute-start.2 = (bf16[128,2176]{1,0:T(8,128)(2,1)}, bf16[128,2176]{1,0:T(8,128)(2,1)S(1)}, u32[]{:S(2)}, u32[]{:S(2)}) collective-permute-start(bf16[128,2176]{1,0:T(8,128)(2,1)} %get-tuple-element.19.first), channel_id=1, source_target_pairs={{0,1},{1,0},{2,3},{3,2},{4,5},{5,4},{6,7},{7,6},{8,9},{9,8},{10,11... | collective-permute-start | bytes 1671176 | tf_op jit(solution)/shard_map/ppermute | solution.py:169
  5.7 13.3 %collective-permute-start.3 = (bf16[1,512,128]{2,1,0:T(8,128)(2,1)}, bf16[1,512,128]{2,1,0:T(8,128)(2,1)S(1)}, u32[]{:S(2)}, u32[]{:S(2)}) collective-permute-start(bf16[1,512,128]{2,1,0:T(8,128)(2,1)} %bitcast.17), channel_id=1, source_target_pairs={{0,4},{1,5},{2,6},{3,7},{4,0},{5,1},{6,2},{7,3},{8,12},{9,13},{10,... | collective-permute-start | bytes 393224 | tf_op jit(solution)/shard_map/ppermute | solution.py:169
  18.6 22.1 %collective-permute-start.1 = (bf16[128,2176]{1,0:T(8,128)(2,1)S(1)}, bf16[128,2176]{1,0:T(8,128)(2,1)S(1)}, u32[]{:S(2)}, u32[]{:S(2)}) collective-permute-start(bf16[128,2176]{1,0:T(8,128)(2,1)S(1)} %collective-permute-done.first), channel_id=1, source_target_pairs={{0,1},{1,0},{2,3},{3,2},{4,5},{5,4},{6,7},{7,6},{8,9},{9,8},{10,11... | collective-permute-start | bytes 1671176 | tf_op jit(solution)/shard_map/ppermute | solution.py:169
  18.6 61.5 %collective-permute-start.11 = (bf16[1,2048,512]{2,1,0:T(8,128)(2,1)}, bf16[1,2048,512]{2,1,0:T(8,128)(2,1)S(1)}, u32[]{:S(2)}, u32[]{:S(2)}) collective-permute-start(bf16[1,2048,512]{2,1,0:T(8,128)(2,1)} %gate0.1), channel_id=1, source_target_pairs={{0,1},{1,0},{2,3},{3,2},{4,5},{5,4},{6,7},{7,6},{8,9},{9,8},{10,11... | collective-permute-start | bytes 6291464 | tf_op jit(solution)/shard_map/ppermute | solution.py:169
  19.1 61.0 %collective-permute-start.12 = (bf16[1,2048,512]{2,1,0:T(8,128)(2,1)}, bf16[1,2048,512]{2,1,0:T(8,128)(2,1)}, u32[]{:S(2)}, u32[]{:S(2)}) collective-permute-start(bf16[1,2048,512]{2,1,0:T(8,128)(2,1)} %up0.1), channel_id=1, source_target_pairs={{0,1},{1,0},{2,3},{3,2},{4,5},{5,4},{6,7},{7,6},{8,9},{9,8},{10,11... | collective-permute-start | bytes 6291464 | tf_op jit(solution)/shard_map/ppermute | solution.py:169
  19.1 61.0 %collective-permute-start.13 = (bf16[1,512,2048]{2,1,0:T(8,128)(2,1)}, bf16[1,512,2048]{2,1,0:T(8,128)(2,1)}, u32[]{:S(2)}, u32[]{:S(2)}) collective-permute-start(bf16[1,512,2048]{2,1,0:T(8,128)(2,1)} %down0.1), channel_id=1, source_target_pairs={{0,1},{1,0},{2,3},{3,2},{4,5},{5,4},{6,7},{7,6},{8,9},{9,8},{10,11... | collective-permute-start | bytes 6291464 | tf_op jit(solution)/shard_map/ppermute | solution.py:169
  21.5 26.6 %collective-permute-start.4 = (bf16[2,512,128]{2,1,0:T(8,128)(2,1)}, bf16[2,512,128]{2,1,0:T(8,128)(2,1)}, u32[]{:S(2)}, u32[]{:S(2)}) collective-permute-start(bf16[2,512,128]{2,1,0:T(8,128)(2,1)} %shard_map.225.refs_0_), channel_id=1, source_target_pairs={{0,8},{1,9},{2,10},{3,11},{4,12},{5,13},{6,14},{7,15},{8,0},{9,1},... | collective-permute-start | bytes 786440 | tf_op jit(solution)/shard_map/ppermute | solution.py:169
  38.6 9.5 %copy-start.11 = (f32[4]{0:T(128)S(1)}, f32[4]{0:T(128)}, u32[]{:S(2)}) copy-start(f32[4]{0:T(128)} %ingate_bias.1) | copy-start | bytes 52
  40.3 7.7 %copy-start.4 = (bf16[12,2048]{1,0:T(8,128)(2,1)S(1)}, bf16[12,2048]{1,0:T(8,128)(2,1)}, u32[]{:S(2)}) copy-start(bf16[12,2048]{1,0:T(8,128)(2,1)} %tokens.5) | copy-start | bytes 147460
  40.3 7.7 %copy-start.8 = (s32[12,6]{0,1:T(8,128)S(1)}, s32[12,6]{0,1:T(8,128)}, u32[]{:S(2)}) copy-start(s32[12,6]{0,1:T(8,128)} %param.38) | copy-start | bytes 868
  40.3 7.7 %copy-start.9 = (f32[12,6]{0,1:T(8,128)S(1)}, f32[12,6]{0,1:T(8,128)}, u32[]{:S(2)}) copy-start(f32[12,6]{0,1:T(8,128)} %param.39) | copy-start | bytes 868
  40.3 7.7 %copy-start.10 = (f32[12,4]{0,1:T(4,128)S(1)}, f32[12,4]{0,1:T(4,128)}, u32[]{:S(2)}) copy-start(f32[12,4]{0,1:T(4,128)} %param.32) | copy-start | bytes 580
  41.7 14.3 %all-to-all-start.1 = ((bf16[4,8,3328]{2,1,0:T(8,128)(2,1)}), bf16[4,8,3328]{2,1,0:T(8,128)(2,1)S(1)}, u32[]{:S(2)}, u32[]{:S(2)}) async-start(bf16[4,8,3328]{2,1,0:T(8,128)(2,1)} %shard_map.221), calls=%async_computation.1 | async-start | bytes 425984 | tf_op jit(solution)/shard_map/all_to_all | solution.py:674
  46.5 8.0 %collective-permute-start.5 = (bf16[2,512,128]{2,1,0:T(8,128)(2,1)S(1)}, bf16[2,512,128]{2,1,0:T(8,128)(2,1)S(1)}, u32[]{:S(2)}, u32[]{:S(2)}) collective-permute-start(bf16[2,512,128]{2,1,0:T(8,128)(2,1)S(1)} %copy-done.5), channel_id=1, source_target_pairs={{0,2},{1,3},{2,0},{3,1},{4,6},{5,7},{6,4},{7,5},{8,10},{9,11},{10,... | collective-permute-start | bytes 786440 | tf_op jit(solution)/shard_map/ppermute | solution.py:169
  48.0 8.0 %collective-permute-start.7 = (bf16[2,512,128]{2,1,0:T(8,128)(2,1)S(1)}, bf16[2,512,128]{2,1,0:T(8,128)(2,1)S(1)}, u32[]{:S(2)}, u32[]{:S(2)}) collective-permute-start(bf16[2,512,128]{2,1,0:T(8,128)(2,1)S(1)} %copy-done.5), channel_id=1, source_target_pairs={{0,1},{1,0},{2,3},{3,2},{4,5},{5,4},{6,7},{7,6},{8,9},{9,8},{10,11... | collective-permute-start | bytes 786440 | tf_op jit(solution)/shard_map/ppermute | solution.py:169
  54.5 7.4 %collective-permute-start.6 = (bf16[2,512,128]{2,1,0:T(8,128)(2,1)}, bf16[2,512,128]{2,1,0:T(8,128)(2,1)S(1)}, u32[]{:S(2)}, u32[]{:S(2)}) collective-permute-start(bf16[2,512,128]{2,1,0:T(8,128)(2,1)} %collective-permute-done.4.refs_1_), channel_id=1, source_target_pairs={{0,2},{1,3},{2,0},{3,1},{4,6},{5,7},{6,4},{7,5},{8,10},{9,11},{10,... | collective-permute-start | bytes 786440 | tf_op jit(solution)/shard_map/ppermute | solution.py:169
  56.0 5.8 %collective-permute-start.8 = (bf16[2,512,128]{2,1,0:T(8,128)(2,1)}, bf16[2,512,128]{2,1,0:T(8,128)(2,1)}, u32[]{:S(2)}, u32[]{:S(2)}) collective-permute-start(bf16[2,512,128]{2,1,0:T(8,128)(2,1)} %collective-permute-done.4.refs_1_), channel_id=1, source_target_pairs={{0,1},{1,0},{2,3},{3,2},{4,5},{5,4},{6,7},{7,6},{8,9},{9,8},{10,11... | collective-permute-start | bytes 786440 | tf_op jit(solution)/shard_map/ppermute | solution.py:169
  61.9 2.5 %collective-permute-start.9 = (bf16[2,512,128]{2,1,0:T(8,128)(2,1)S(1)}, bf16[2,512,128]{2,1,0:T(8,128)(2,1)S(1)}, u32[]{:S(2)}, u32[]{:S(2)}) collective-permute-start(bf16[2,512,128]{2,1,0:T(8,128)(2,1)S(1)} %collective-permute-done.5.refs_2_), channel_id=1, source_target_pairs={{0,1},{1,0},{2,3},{3,2},{4,5},{5,4},{6,7},{7,6},{8,9},{9,8},{10,11... | collective-permute-start | bytes 786440 | tf_op jit(solution)/shard_map/ppermute | solution.py:169
  61.9 2.5 %collective-permute-start.10 = (bf16[2,512,128]{2,1,0:T(8,128)(2,1)S(1)}, bf16[2,512,128]{2,1,0:T(8,128)(2,1)S(1)}, u32[]{:S(2)}, u32[]{:S(2)}) collective-permute-start(bf16[2,512,128]{2,1,0:T(8,128)(2,1)S(1)} %collective-permute-done.6.refs_3_), channel_id=1, source_target_pairs={{0,1},{1,0},{2,3},{3,2},{4,5},{5,4},{6,7},{7,6},{8,9},{9,8},{10,11... | collective-permute-start | bytes 786440 | tf_op jit(solution)/shard_map/ppermute | solution.py:169
  64.4 15.7 %copy-start = (bf16[1,2048,512]{2,1,0:T(8,128)(2,1)S(1)}, bf16[1,2048,512]{2,1,0:T(8,128)(2,1)}, u32[]{:S(2)}) copy-start(bf16[1,2048,512]{2,1,0:T(8,128)(2,1)} %gate0.1) | copy-start | bytes 6291460
  64.4 15.7 %copy-start.1 = (bf16[1,2048,512]{2,1,0:T(8,128)(2,1)S(1)}, bf16[1,2048,512]{2,1,0:T(8,128)(2,1)}, u32[]{:S(2)}) copy-start(bf16[1,2048,512]{2,1,0:T(8,128)(2,1)} %up0.1) | copy-start | bytes 6291460
  64.4 15.7 %copy-start.2 = (bf16[1,512,2048]{2,1,0:T(8,128)(2,1)S(1)}, bf16[1,512,2048]{2,1,0:T(8,128)(2,1)}, u32[]{:S(2)}) copy-start(bf16[1,512,2048]{2,1,0:T(8,128)(2,1)} %down0.1) | copy-start | bytes 6291460
  85.6 11.1 %all-to-all-start.3 = ((bf16[8,8,1536]{2,1,0:T(8,128)(2,1)}), bf16[8,8,1536]{2,1,0:T(8,128)(2,1)S(1)}, u32[]{:S(2)}, u32[]{:S(2)}) async-start(bf16[8,8,1536]{2,1,0:T(8,128)(2,1)} %bitcast.9), calls=%async_computation.3 | async-start | bytes 393216 | tf_op jit(solution)/shard_map/all_to_all | solution.py:748
  (8 other events, 18.3 us)
